TPU v7x, 256 devices: a whole 4x4x8 slice. The times are simulated.
256 devices in a mesh: sp: 64 (over z, x, core), tp: 4 (over y).
Axes of the slice: x: 4, y: 4, z: 8, core: 2. Of those that a mesh axis runs over, the one named last changes fastest.
Arguments:
- tokens: bfloat16 [16384, 2048], P(('sp', 'tp')), may hold values from -6 to 6
- norm_gain: float32 [2048], replicated, may hold values from 0.1 to 1.9
- w_glu_a: bfloat16 [2048, 2048], P(None, 'tp'), may hold values from -0.125 to 0.125
- w_glu_b: bfloat16 [2048, 2048], P(None, 'tp'), may hold values from -0.125 to 0.125
- conv_taps: float32 [31, 2048], P(None, 'tp'), may hold values from -6 to 6
- ln_gain: float32 [2048], P('tp'), may hold values from 0.1 to 1.9
- w_query: bfloat16 [2048, 2048], P(None, 'tp'), may hold values from -0.125 to 0.125
- w_key: bfloat16 [2048, 512], P(None, 'tp'), may hold values from -0.125 to 0.125
- w_value: bfloat16 [2048, 512], P(None, 'tp'), may hold values from -0.125 to 0.125
- query_gain: float32 [16, 128], P('tp'), may hold values from 1 to 40
- key_gain: float32 [4, 128], P('tp'), may hold values from 0.1 to 1.9
- lam_head: float32 [16], P('tp'), may hold values from 0.3 to 0.8
- sub_gain: float32 [128], replicated, may hold values from 0.1 to 1.9
- w_out_conv: bfloat16 [2048, 2048], P('tp'), may hold values from -0.09375 to 0.09375
- w_out_attn: bfloat16 [2048, 2048], P('tp'), may hold values from -0.09375 to 0.09375
Outputs:
- mixed: bfloat16 [16384, 2048], P(('sp', 'tp'))
- log_sums: float32 [2, 16, 16384], P(None, 'tp', 'sp')
All inputs are finite; a program needn't handle non-finite values.
Results may differ from a plain program's by a relative error of at most 0.015.
The roundings to bfloat16 on the way count: a program that leaves them out, or rounds other values in their place, can miss the bound.
Values may be sent and summed in bfloat16 or wider, within the bound.
No kernel may reach another device: no remote copies, remote signals or barrier semaphores. Data moves between devices by JAX's collectives and lax.ppermute only.
A program may use at most 128 MiB of HBM per device.

v0:
```python
import jax
import jax.numpy as jnp
from jax import lax
from jax.sharding import PartitionSpec as P

KW = 31


def shifted(value, axis, steps):
    count = lax.axis_size(axis)
    leading, last = (max(0, -steps), min(count, count - steps))
    return lax.ppermute(value, axis, [(source, source + steps) for source in range(leading, last)])


def sent_to_all(value, axis):
    count = lax.axis_size(axis)
    return lax.all_to_all(
        jnp.broadcast_to(value[None], (count, *value.shape)), axis, 0, 0, tiled=True
    )


def taken_together(value, axis):
    everything = sent_to_all(value, axis)
    return jnp.sum(everything, axis=0)


def packed_total(arrays, axis):
    ravelled, at, outs = (jnp.concatenate([a.reshape(-1) for a in arrays]), 0, [])
    subtotal = taken_together(ravelled, axis)
    for a in arrays:
        outs.append(subtotal[at : at + a.size].reshape(a.shape))
        at += a.size
    return tuple(outs)


def sent_together(arrays, axis, dim, along):
    widths = [a.shape[along] for a in arrays]
    both = jnp.concatenate(arrays, axis=along)
    filled = lax.all_gather(both, axis, axis=dim, tiled=True)
    return tuple(jnp.split(filled, [sum(widths[:k]) for k in range(1, len(widths))], axis=along))


def cut_along(value, dim, count):
    before, after = (value.shape[:dim], value.shape[dim + 1 :])
    return jnp.moveaxis(value.reshape(*before, count, -1, *after), dim, 0)


def sum_at_owner(value, axis, dim):
    count = lax.axis_size(axis)
    blocks = lax.all_to_all(cut_along(value, dim, count), axis, 0, 0, tiled=True)
    return jnp.sum(blocks.astype(jnp.float32), axis=0)


def rms_scale(inputs_arr, gain_vec, epsilon):
    return (
        inputs_arr
        * lax.rsqrt(jnp.mean(inputs_arr * inputs_arr, axis=-1, keepdims=True) + epsilon)
        * gain_vec
    )


def attend_rows(totals, key_rows, value_rows, key_start, query_start, queries, kv_local):
    row_count = key_rows.shape[0]
    head_dim = queries.shape[4]
    key_grid = key_rows.reshape(row_count, kv_local, 2, head_dim)
    value_grid = value_rows.reshape(row_count, kv_local, -1)
    run_max, run_sum, run_acc = totals
    scores = jnp.einsum(
        "tkgmd,rkmd->kgmtr", queries, key_grid, preferred_element_type=jnp.float32
    ) * head_dim ** (-0.5)
    query_pos = query_start + jnp.arange(queries.shape[0], dtype=jnp.int32)
    key_pos = key_start + jnp.arange(row_count, dtype=jnp.int32)
    visible = (key_pos[None, :] <= query_pos[:, None]) & (key_pos[None, :] >= 0)
    scores = jnp.where(visible, scores, -1e30)
    new_max = jnp.maximum(run_max, jnp.max(scores, axis=-1))
    rescale = jnp.exp(run_max - new_max)
    weights = jnp.where(visible, jnp.exp(scores - new_max[..., None]), 0.0)
    new_sum = run_sum * rescale + jnp.sum(weights, axis=-1)
    contrib = jnp.einsum(
        "kgmtr,rkv->kgmtv",
        weights.astype(jnp.bfloat16),
        value_grid,
        preferred_element_type=jnp.float32,
    )
    new_acc = run_acc * rescale[..., None] + contrib
    return (new_max, new_sum, new_acc)


def attend_span(totals, key_rows, value_rows, query_start, queries, kv_local, shard_rows):
    total_rows = key_rows.shape[0]
    shard_count = total_rows // shard_rows
    per_step = 1
    for candidate in range(1, shard_count + 1):
        if shard_count % candidate == 0 and candidate * shard_rows <= 1024:
            per_step = candidate
    step_rows = per_step * shard_rows
    step_count = shard_count // per_step
    key_blocks = key_rows.reshape(step_count, step_rows, key_rows.shape[1])
    value_blocks = value_rows.reshape(step_count, step_rows, value_rows.shape[1])

    def one_step(running, inputs):
        key_blk, value_blk, blk_idx = inputs
        return (
            attend_rows(
                running, key_blk, value_blk, blk_idx * step_rows, query_start, queries, kv_local
            ),
            None,
        )

    final_state, unused = lax.scan(
        one_step, totals, (key_blocks, value_blocks, jnp.arange(step_count, dtype=jnp.int32))
    )
    return final_state


def empty_state(kv_local, group_size, row_count, value_dim):
    return (
        jnp.full((kv_local, group_size, 2, row_count), -1e30, jnp.float32),
        jnp.zeros((kv_local, group_size, 2, row_count), jnp.float32),
        jnp.zeros((kv_local, group_size, 2, row_count, value_dim), jnp.float32),
    )


def finish_heads(totals, lam_head, sub_gain, kv_local, group_size):
    run_max, run_sum, run_acc = totals
    row_count = run_max.shape[3]
    mixed_maps = run_acc / run_sum[..., None]
    lam_grid = lam_head.reshape(kv_local, group_size)[:, :, None, None]
    diff_out = mixed_maps[:, :, 0] - lam_grid * mixed_maps[:, :, 1]
    head_out = rms_scale(diff_out, sub_gain, 1e-06).astype(jnp.bfloat16)
    attn_rows = head_out.transpose(2, 0, 1, 3).reshape(row_count, -1)
    log_rows = (
        (run_max + jnp.log(run_sum)).reshape(kv_local * group_size, 2, row_count).transpose(1, 0, 2)
    )
    return (attn_rows, log_rows)


def on_device(
    tokens,
    norm_gain,
    w_glu_a,
    w_glu_b,
    conv_taps,
    ln_gain,
    w_query,
    w_key,
    w_value,
    query_gain,
    key_gain,
    lam_head,
    sub_gain,
    w_out_conv,
    w_out_attn,
):
    tp_count = lax.axis_size("tp")
    tok_dev = tokens.shape[0] * tp_count
    seq_offset = lax.axis_index("sp") * tok_dev
    conv_local = w_glu_a.shape[1]
    head_local = lam_head.shape[0]
    kv_local = key_gain.shape[0]
    head_dim = key_gain.shape[1] // 2
    query_cols = w_query.shape[1]
    key_cols = w_key.shape[1]
    normed = rms_scale(tokens.astype(jnp.float32), norm_gain, 1e-06).astype(jnp.bfloat16)
    rows_block = lax.all_gather(normed, "tp", axis=0, tiled=True)
    glu_a = jnp.dot(rows_block, w_glu_a, preferred_element_type=jnp.float32)
    glu_b = jnp.dot(rows_block, w_glu_b, preferred_element_type=jnp.float32)
    gated_part = (glu_a * jax.nn.sigmoid(glu_b)).astype(jnp.bfloat16)
    query_part = jnp.dot(rows_block, w_query, preferred_element_type=jnp.float32).reshape(
        -1, head_local, 2, head_dim
    )
    query_part = (
        rms_scale(query_part, query_gain.reshape(head_local, 2, head_dim), 1e-06)
        .astype(jnp.bfloat16)
        .reshape(-1, query_cols)
    )
    key_part = jnp.dot(rows_block, w_key, preferred_element_type=jnp.float32).reshape(
        -1, kv_local, 2, head_dim
    )
    key_part = (
        rms_scale(key_part, key_gain.reshape(kv_local, 2, head_dim), 1e-06)
        .astype(jnp.bfloat16)
        .reshape(-1, key_cols)
    )
    value_part = jnp.dot(rows_block, w_value, preferred_element_type=jnp.float32).astype(
        jnp.bfloat16
    )
    projected = jnp.concatenate([gated_part, query_part, key_part, value_part], axis=1)
    group_size = head_local // kv_local
    gated_rows = projected[:, :conv_local]
    queries = projected[:, conv_local : conv_local + query_cols].reshape(
        tok_dev, kv_local, group_size, 2, head_dim
    )
    key_rows = projected[:, conv_local + query_cols : conv_local + query_cols + key_cols]
    value_rows = projected[:, conv_local + query_cols + key_cols :]
    value_dim = value_rows.shape[1] // kv_local
    prev_rows = shifted(gated_rows[tok_dev - (KW - 1) :], "sp", 1)
    padded = jnp.concatenate([prev_rows, gated_rows], axis=0)
    conv_sum = jnp.zeros((tok_dev, conv_local), jnp.float32)
    for tap_idx in range(KW):
        conv_sum = conv_sum + conv_taps[tap_idx] * padded[tap_idx : tap_idx + tok_dev].astype(
            jnp.float32
        )
    chan_total = conv_local * tp_count
    sum_one, sum_two = packed_total(
        (jnp.sum(conv_sum, axis=1), jnp.sum(conv_sum * conv_sum, axis=1)), "tp"
    )
    mean_val = (sum_one / chan_total)[:, None]
    mean_sq = (sum_two / chan_total)[:, None]
    conv_out = jax.nn.silu(
        (conv_sum - mean_val) * lax.rsqrt(mean_sq - mean_val * mean_val + 1e-05) * ln_gain
    ).astype(jnp.bfloat16)
    start_state = empty_state(kv_local, group_size, tok_dev, value_dim)
    pieces = sent_together((key_rows, value_rows), "sp", 0, 1)
    totals = lax.cond(
        jnp.int32(0) <= seq_offset + tok_dev - 1,
        lambda running: attend_span(
            running, pieces[0], pieces[1], seq_offset, queries, kv_local, tok_dev
        ),
        lambda running: running,
        start_state,
    )
    attn_out, log_sums = finish_heads(totals, lam_head, sub_gain, kv_local, group_size)
    out_part = jnp.dot(conv_out, w_out_conv, preferred_element_type=jnp.float32)
    out_part = out_part + jnp.dot(attn_out, w_out_attn, preferred_element_type=jnp.float32)
    mixed = sum_at_owner(
        lax.optimization_barrier(out_part.astype(jnp.bfloat16))
        .astype(jnp.float32)
        .astype(jnp.bfloat16),
        "tp",
        0,
    )
    return (mixed.astype(jnp.bfloat16), log_sums)


def solution(mesh):
    return jax.shard_map(
        on_device,
        mesh=mesh,
        in_specs=(
            P(("sp", "tp"), None),
            P(),
            P(None, "tp"),
            P(None, "tp"),
            P(None, "tp"),
            P("tp"),
            P(None, "tp"),
            P(None, "tp"),
            P(None, "tp"),
            P("tp", None),
            P("tp", None),
            P("tp"),
            P(),
            P("tp", None),
            P("tp", None),
        ),
        out_specs=(P(("sp", "tp"), None), P(None, "tp", "sp")),
        check_vma=False,
    )
```

profile of v0, /device:TPU:34, one launch (start us, length us, event | category | flops | bytes accessed | tf_op | source)
XLA Modules:
  0.0 382.8 jit_solution(15534507754161818594)
XLA Ops:
  10.4 29.4 %all-gather.3.cloned.1.call-done = bf16[256,2048]{1,0:T(8,128)(2,1)} async-done(((bf16[64,2048]{1,0:T(8,128)(2,1)}), bf16[256,2048]{1,0:T(8,128)(2,1)}) %all-gather.3.cloned.1.call-update) | async-done | bytes 1048592 | tf_op jit(solution)/shard_map/all_gather | solution.py:165
  45.7 3.4 fusion.69
  59.6 3.5 fusion.65
  63.7 3.4 all-to-all-start
  67.3 5.1 %all-to-all-done = f32[4,1,512]{2,1,0:T(1,128)S(1)} async-done(((f32[4,1,512]{2,1,0:T(1,128)}), f32[4,1,512]{2,1,0:T(1,128)S(1)}, u32[]{:S(2)}, u32[]{:S(2)}) %all-to-all-start) | async-done | bytes 8224 | tf_op jit(solution)/shard_map/all_to_all | solution.py:17
  75.3 56.1 %all-gather.5.cloned.1.call-done = bf16[16384,256]{0,1:T(8,128)(2,1)} async-done(((bf16[256,256]{0,1:T(8,128)(2,1)}), bf16[16384,256]{0,1:T(8,128)(2,1)}) %all-gather.5.cloned.1.call-update) | async-done | bytes 8388624 | tf_op jit(solution)/shard_map/all_gather | solution.py:39
  131.4 219.6 %conditional.1 = (f32[1,4,2,256]{3,1,2,0:T(4,128)}, f32[1,4,2,256]{3,1,2,0:T(4,128)}, f32[1,4,2,256,128]{3,4,1,2,0:T(8,128)}, f32[1,4,2,256]{3,1,2,0:T(4,128)S(1)}) conditional(s32[]{:T(128)} %convert_element_type.183, () %tuple.20, (bf16[16384,256]{0,1:T(8,128)(2,1)}, s32[]{:T(128)}, bf16[256,1,4,2,64]{0,4,3,2,1:T(8,128)(2,1)S(1)}) %tuple.21), branch_computations={%region_6.7_spmd, %region_7.12_spmd} | conditional | flops 825507072 | bytes 74617264 | solution.py:215
  131.4 11.9 %copy.46 = bf16[16384,256]{1,0:T(8,128)(2,1)} copy(bf16[16384,256]{0,1:T(8,128)(2,1)} %get-tuple-element.135) | data formatting | bytes 16777216 | tf_op jit(solution)/shard_map
  143.3 5.7 %fusion.66 = (bf16[16384,128]{1,0:T(8,128)(2,1)}, bf16[16384,128]{1,0:T(8,128)(2,1)}) fusion(bf16[16384,256]{1,0:T(8,128)(2,1)} %copy.46), kind=kLoop, calls=%fused_computation.139 | loop fusion | bytes 16777216 | tf_op jit(solution)/shard_map/split | solution.py:40
  149.1 198.6 %while.14 = (s32[]{:T(128)}, f32[1,4,2,256]{3,1,2,0:T(4,128)}, f32[1,4,2,256]{3,1,2,0:T(4,128)}, f32[1,4,2,256,128]{4,3,2,1,0:T(8,128)}, s32[16]{0:T(128)S(1)}, ...) while((s32[]{:T(128)}, f32[1,4,2,256]{3,1,2,0:T(4,128)}, ...), condition=%wide.region_11.11_spmd.clone, body=%wide.region_8.10_spmd.clone.sunk | while | flops 825507072 | bytes 38424812 | solution.py:110
  156.3 2.9 fusion.97
  168.8 2.9 fusion.97
  181.3 2.9 fusion.97
  193.8 2.9 fusion.97
  206.3 2.9 fusion.97
  218.8 2.9 fusion.97
  231.3 2.9 fusion.97
  243.8 2.9 fusion.97
  256.2 2.9 fusion.97
  268.7 2.9 fusion.97
  293.7 2.9 fusion.97
  306.2 2.9 fusion.97
  355.2 4.3 %all-to-all-start.1 = ((bf16[4,64,2048]{2,1,0:T(8,128)(2,1)}), bf16[4,64,2048]{2,1,0:T(8,128)(2,1)S(1)}, u32[]{:S(2)}, u32[]{:S(2)}) async-start(bf16[4,64,2048]{2,1,0:T(8,128)(2,1)} %bitcast.158), calls=%async_computation.1 | async-start | bytes 2097152 | tf_op jit(solution)/shard_map/all_to_all | solution.py:50
  360.8 14.2 %all-to-all-done.1 = bf16[4,64,2048]{2,1,0:T(8,128)(2,1)S(1)} async-done(((bf16[4,64,2048]{2,1,0:T(8,128)(2,1)}), bf16[4,64,2048]{2,1,0:T(8,128)(2,1)S(1)}, u32[]{:S(2)}, u32[]{:S(2)}) %all-to-all-start.1) | async-done | bytes 1048608 | tf_op jit(solution)/shard_map/all_to_all | solution.py:50
  (340 shorter events, 184.9 us)
Async XLA Ops:
  7.2 65.2 %copy-start = (bf16[512,2048]{1,0:T(8,128)(2,1)S(1)}, bf16[512,2048]{1,0:T(8,128)(2,1)}, u32[]{:S(2)}) copy-start(bf16[512,2048]{1,0:T(8,128)(2,1)} %param.32) | copy-start | bytes 6291460
  7.2 37.8 %copy-start.10 = (f32[4,128]{1,0:T(4,128)S(1)}, f32[4,128]{1,0:T(4,128)}, u32[]{:S(2)}) copy-start(f32[4,128]{1,0:T(4,128)} %param.28) | copy-start | bytes 6148
  7.2 37.9 %copy-start.8 = (f32[31,512]{1,0:T(8,128)S(1)}, f32[31,512]{1,0:T(8,128)}, u32[]{:S(2)}) copy-start(f32[31,512]{1,0:T(8,128)} %param.23) | copy-start | bytes 190468
  7.2 32.5 %all-gather.3.cloned.1.call-start = ((), (), s32[]{:S(2)}) async-start(), calls=%async_computation.2 | async-start | bytes 1310720 | tf_op jit(solution)/shard_map/all_gather | solution.py:165
  10.3 121.0 %all-gather.5.cloned.1.call-start = ((), (), s32[]{:S(2)}) async-start(), calls=%async_computation.3 | async-start | bytes 8519680 | tf_op jit(solution)/shard_map/all_gather | solution.py:39
  39.7 6.0 %copy-start.1 = (bf16[256,2048]{1,0:T(8,128)(2,1)S(1)}, bf16[256,2048]{1,0:T(8,128)(2,1)}, u32[]{:S(2)}) copy-start(bf16[256,2048]{1,0:T(8,128)(2,1)} %all-gather.3.cloned.1.call-done) | copy-start | bytes 3145732
  51.1 5.2 %copy-start.4 = (f32[256,512]{0,1:T(8,128)S(1)}, f32[256,512]{0,1:T(8,128)}, u32[]{:S(2)}) copy-start(f32[256,512]{0,1:T(8,128)} %copy.45) | copy-start | bytes 1572868
  54.4 5.2 %collective-permute-start = (bf16[30,512]{1,0:T(8,128)(2,1)S(1)}, bf16[30,512]{1,0:T(8,128)(2,1)S(1)}, u32[]{:S(2)}, u32[]{:S(2)}) collective-permute-start(bf16[30,512]{1,0:T(8,128)(2,1)S(1)} %slice.264), channel_id=1, source_target_pairs={{0,4},{4,8},{8,12},{12,16},{16,20},{20,24},{24,28},{28,32},{32,36}... | collective-permute-start | bytes 92168 | tf_op jit(solution)/shard_map/ppermute | solution.py:12
  63.7 8.7 %all-to-all-start = ((f32[4,1,512]{2,1,0:T(1,128)}), f32[4,1,512]{2,1,0:T(1,128)S(1)}, u32[]{:S(2)}, u32[]{:S(2)}) async-start(f32[4,1,512]{2,1,0:T(1,128)} %broadcast_in_dim.37), calls=%async_computation | async-start | bytes 16384 | tf_op jit(solution)/shard_map/all_to_all | solution.py:17
  131.4 221.1 %copy-start.9 = (f32[4]{0:T(128)S(1)}, f32[4]{0:T(128)}, u32[]{:S(2)}) copy-start(f32[4]{0:T(128)} %param.30) | copy-start | bytes 52
  131.4 221.3 %copy-start.11 = (f32[128]{0:T(128)S(1)}, f32[128]{0:T(128)}, u32[]{:S(2)}) copy-start(f32[128]{0:T(128)} %param.31) | copy-start | bytes 1540
  165.1 3.7 copy-start.6
  177.6 3.7 copy-start.6
  190.1 3.7 copy-start.6
  202.6 3.7 copy-start.6
  215.1 3.7 copy-start.6
  227.6 3.7 copy-start.6
  240.1 3.7 copy-start.6
  252.6 3.7 copy-start.6
  265.1 3.7 copy-start.6
  315.0 3.7 copy-start.6
  327.5 3.7 copy-start.6
  340.0 3.7 copy-start.6
  355.2 19.8 %all-to-all-start.1 = ((bf16[4,64,2048]{2,1,0:T(8,128)(2,1)}), bf16[4,64,2048]{2,1,0:T(8,128)(2,1)S(1)}, u32[]{:S(2)}, u32[]{:S(2)}) async-start(bf16[4,64,2048]{2,1,0:T(8,128)(2,1)} %bitcast.158), calls=%async_computation.1 | async-start | bytes 2097152 | tf_op jit(solution)/shard_map/all_to_all | solution.py:50
  (23 other events, 36.6 us)
Sparse Core Ops, SparseCore 0:
  10.4 29.2 all-gather.2
  45.1 86.2 all-gather.4
where the time goes:
time: 387 us; the launch traced here: 383 us
  waiting for transfers between devices  107 us (28%)
  other arithmetic  86.7 us (22%)
  matrix products  84.3 us (22%)
  local copies, waits for them, and re-layouts  69.5 us (18%)
  between operations  14.3 us (4%)
  loops' own time  11.6 us (3%)
  starting transfers between devices  9.72 us (3%)
    all_gather x1, waiting for transfers between devices, sent_together(): filled = lax.all_gather(both, axis, axis=dim, tiled=True)  56.1 us
    dot_general x16, matrix products, attend_rows(): jnp.einsum('kgmtr,rkv->kgmtv', weights.astype(jnp.bfloat16), value_grid,...  46.7 us
    another operation x16, other arithmetic  37.4 us
    all_gather x1, waiting for transfers between devices, on_device(): rows_block = lax.all_gather(normed, 'tp', axis=0, tiled=True)  29.4 us
    dynamic_slice x48, local copies, waits for them, and re-layouts, attend_span(): lax.scan(one_step, totals, (key_blocks, value_blocks, jnp.arange(step_cou...  27.6 us
    dot_general x16, matrix products, attend_rows(): jnp.einsum('tkgmd,rkmd->kgmtr', queries, key_grid, preferred_element_type...  22.6 us
    add x16, other arithmetic, attend_rows(): new_sum = run_sum * rescale + jnp.sum(weights, axis=-1)  20.7 us
    while x80, local copies, waits for them, and re-layouts  15.5 us
  transfers between devices with their start and end apart: 5, of which 5 were waited for; matrix products, arithmetic and copies ran while one was open for 5% of the time, Pallas kernels for 0%

commit v1 on v0

v1 whole, which is shorter than its diff:
```python
import functools

import jax
import jax.numpy as jnp
from jax import lax
from jax.experimental import pallas as pl
from jax.experimental.pallas import tpu as pltpu
from jax.sharding import PartitionSpec as P

KW = 31
NEG = -1e30
LOG2E = 1.4426950408889634
LN2 = 0.6931471805599453
UNROLL = 4


def sp_table(move):
    table = []
    for index in range(64):
        z, x, core = index // 8, (index // 2) % 4, index % 2
        nz, nx, nc = move(z, x, core)
        table.append((index, (nz % 8) * 8 + (nx % 4) * 2 + nc))
    return table


def sp_send(value, move):
    return lax.ppermute(value, "sp", sp_table(move))


def shifted(value, axis, steps):
    count = lax.axis_size(axis)
    leading, last = (max(0, -steps), min(count, count - steps))
    return lax.ppermute(value, axis, [(source, source + steps) for source in range(leading, last)])


def sent_to_all(value, axis):
    count = lax.axis_size(axis)
    return lax.all_to_all(
        jnp.broadcast_to(value[None], (count, *value.shape)), axis, 0, 0, tiled=True
    )


def rms_scale(inputs_arr, gain_vec, epsilon):
    return (
        inputs_arr
        * lax.rsqrt(jnp.mean(inputs_arr * inputs_arr, axis=-1, keepdims=True) + epsilon)
        * gain_vec
    )


def chunk_refs(pieces):
    return [(ref, row) for ref in pieces for row in range(0, ref.shape[0], 512)]


def slab_pass(chunks, q_ref, stats_ref, o_ref, s_refs, bias_ref):
    units = q_ref.shape[0]

    def score(unit, s_ref, at):
        ref, row = chunks[at]
        keys = ref[row : row + 256, :]
        s = jnp.dot(
            jnp.concatenate([keys, keys], axis=1), q_ref[unit], preferred_element_type=jnp.float32
        )
        if bias_ref is not None:
            s = s + bias_ref[unit // (units // 2), at * 256 : at * 256 + 256, :]
        s_ref[at * 256 : at * 256 + 256, :] = s
        return jnp.max(s.reshape(32, 8, 256), axis=0)

    def both(now, s_now, top, later, s_later):
        m_prev = stats_ref[now, 0:1, :]
        m_new = jnp.maximum(m_prev, jnp.max(top, axis=0, keepdims=True))
        alpha = jnp.exp2(m_prev - m_new)
        total, out, next_top = None, None, None
        for at, (ref, row) in enumerate(chunks):
            part = score(later, s_later, at)
            next_top = part if next_top is None else jnp.maximum(next_top, part)
            p = jnp.exp2(s_now[at * 256 : at * 256 + 256, :] - m_new)
            part = jnp.sum(p.reshape(32, 8, 256), axis=0)
            total = part if total is None else total + part
            vt = jnp.concatenate(
                [ref[row + 256 : row + 384, :], ref[row + 384 : row + 512, :]], axis=1
            )
            part = jnp.dot(vt, p.astype(jnp.bfloat16), preferred_element_type=jnp.float32)
            out = part if out is None else out + part
        stats_ref[now, 0:1, :] = m_new
        l_new = stats_ref[now, 1:2, :] * alpha + jnp.sum(total, axis=0, keepdims=True)
        stats_ref[now, 1:2, :] = l_new
        o_ref[now] = o_ref[now] * alpha + out
        return next_top

    top = None
    for at in range(len(chunks)):
        part = score(0, s_refs[0], at)
        top = part if top is None else jnp.maximum(top, part)

    def some(i, top):
        for j in range(UNROLL):
            unit = UNROLL * i + j
            later = jnp.minimum(unit + 1, units - 1)
            top = both(unit, s_refs[j % 2], top, later, s_refs[(j + 1) % 2])
        return top

    lax.fori_loop(0, units // UNROLL, some, top)


def spread_queries(q_in, q_ref):
    scale = LOG2E * q_in.shape[1] ** (-0.5)
    zero = jnp.zeros((64, 256), jnp.bfloat16)
    for unit in range(q_in.shape[0]):
        scaled = q_in[unit].astype(jnp.float32) * scale
        high = scaled.astype(jnp.bfloat16)
        low = (scaled - high.astype(jnp.float32)).astype(jnp.bfloat16)
        at = 64 * (unit % 2)
        for first, part in ((0, high), (128, low)):
            q_ref[unit, first + at : first + at + 64, :] = part
            q_ref[unit, first + 64 - at : first + 128 - at, :] = zero


def first_kernel(
    where_ref, q_in, own_ref, left_ref, right_ref, far_ref, stats_ref, o_ref, q_ref, s_a, s_b, bias_ref
):
    spread_queries(q_in, q_ref)
    x, core = where_ref[1], where_ref[2]
    units = q_ref.shape[0]
    stats_ref[...] = jnp.zeros_like(stats_ref)
    for unit in range(units):
        stats_ref[unit, 0:1, :] = jnp.full((1, 256), NEG, jnp.float32)
    o_ref[...] = jnp.zeros_like(o_ref)
    key_at = lax.broadcasted_iota(jnp.int32, (256, 256), 0)
    query_at = lax.broadcasted_iota(jnp.int32, (256, 256), 1)
    bias_ref[0, 0:256, :] = jnp.where(key_at <= query_at, 0.0, NEG)
    bias_ref[1, 0:256, :] = jnp.full((256, 256), jnp.where(core == 0, 0.0, NEG), jnp.float32)
    for at, step in ((1, 3), (2, 1), (3, 2)):
        seen = jnp.where(lax.rem(x + step, 4) < x, 0.0, NEG)
        for which in range(2):
            bias_ref[which, at * 256 : at * 256 + 256, :] = jnp.full((256, 256), seen, jnp.float32)
    chunks = chunk_refs((own_ref, left_ref, right_ref, far_ref))
    slab_pass(chunks, q_ref, stats_ref, o_ref, (s_a, s_b), bias_ref)


def slab_kernel(
    step, where_ref, q_in, a_ref, b_ref, stats_in, o_in, stats_ref, o_ref, q_ref, s_a, s_b
):
    z = where_ref[0]
    spread_queries(q_in, q_ref)

    def go(*pieces):
        slab_pass(chunk_refs(pieces), q_ref, stats_ref, o_ref, (s_a, s_b), None)

    if step == 4:
        pl.when(z >= 4)(lambda: go(a_ref, b_ref))
    else:
        pl.when(z >= step)(lambda: go(a_ref))
        pl.when(z + step >= 8)(lambda: go(b_ref))


def attend(where, q, pieces, state, step):
    units = q.shape[0]
    shapes = ((units, 8, 256), (units, 128, 256))
    vmem = pl.BlockSpec(memory_space=pltpu.VMEM)
    smem = pl.BlockSpec(memory_space=pltpu.SMEM)
    scratch = [pltpu.VMEM((units, 256, 256), jnp.bfloat16), pltpu.VMEM((1024, 256), jnp.float32), pltpu.VMEM((1024, 256), jnp.float32)]
    if step == 0:
        body, args, aliases = first_kernel, (where, q, *pieces), {}
        scratch.append(pltpu.VMEM((2, 1024, 256), jnp.float32))
        keys = 1024
    else:
        body, args = functools.partial(slab_kernel, step), (where, q, *pieces, *state)
        aliases = {4: 0, 5: 1}
        keys = sum(p.shape[0] for p in pieces) // 2
    return pl.pallas_call(
        body,
        out_shape=tuple(STATE(s) for s in shapes),
        in_specs=[smem] + [vmem] * (len(args) - 1),
        out_specs=(vmem, vmem),
        scratch_shapes=scratch,
        input_output_aliases=aliases,
        compiler_params=pltpu.CompilerParams(vmem_limit_bytes=24 << 20),
        cost_estimate=pl.CostEstimate(
            flops=2 * keys * 256 * units * 256, bytes_accessed=6 << 20, transcendentals=0
        ),
        name=f"attend_{step}",
    )(*args)


def STATE(shape):
    return pltpu.VMEM(shape, jnp.float32)


def on_device(
    tokens,
    norm_gain,
    w_glu_a,
    w_glu_b,
    conv_taps,
    ln_gain,
    w_query,
    w_key,
    w_value,
    query_gain,
    key_gain,
    lam_head,
    sub_gain,
    w_out_conv,
    w_out_attn,
):
    tp_count = lax.axis_size("tp")
    tok_dev = tokens.shape[0] * tp_count
    conv_local = w_glu_a.shape[1]
    heads = lam_head.shape[0]
    head_dim = key_gain.shape[1] // 2
    sp = lax.axis_index("sp")
    where = jnp.stack([sp // 8, (sp // 2) % 4, sp % 2]).astype(jnp.int32)

    normed = rms_scale(tokens.astype(jnp.float32), norm_gain, 1e-06).astype(jnp.bfloat16)
    rows_block = sent_to_all(normed, "tp").reshape(tok_dev, -1)

    key_part = jnp.dot(rows_block, w_key, preferred_element_type=jnp.float32).reshape(
        tok_dev, 2, head_dim
    )
    key_part = (
        rms_scale(key_part, key_gain.reshape(2, head_dim), 1e-06)
        .astype(jnp.bfloat16)
        .reshape(tok_dev, 2 * head_dim)
    )
    value_part = jnp.dot(rows_block, w_value, preferred_element_type=jnp.float32).astype(
        jnp.bfloat16
    )
    value_t = value_part.T
    own = jnp.concatenate([key_part, value_t[:, :128], value_t[:, 128:]], axis=0)

    left = sp_send(own, lambda z, x, c: (z, x + 1, c))
    right = sp_send(own, lambda z, x, c: (z, x - 1, c))
    far = sp_send(own, lambda z, x, c: (z, x + 2, c))
    slab = jnp.concatenate([own, left, right, far], axis=0)

    query_t = jnp.dot(rows_block, w_query, preferred_element_type=jnp.float32).T.reshape(
        heads * 2, head_dim, tok_dev
    )
    query_t = (
        query_t
        * lax.rsqrt(jnp.mean(query_t * query_t, axis=1, keepdims=True) + 1e-06)
        * query_gain.reshape(heads * 2, head_dim, 1)
    ).astype(jnp.bfloat16)
    partner_q = sp_send(query_t.reshape(heads * 128, tok_dev), lambda z, x, c: (z, x, 1 - c))
    both_q = jnp.concatenate([query_t, partner_q.reshape(query_t.shape)], axis=0)

    up = sp_send(slab, lambda z, x, c: (z + 1, x, c))
    down = sp_send(slab, lambda z, x, c: (z - 1, x, c))

    glu_a = jnp.dot(rows_block, w_glu_a, preferred_element_type=jnp.float32)
    glu_b = jnp.dot(rows_block, w_glu_b, preferred_element_type=jnp.float32)
    gated_rows = (glu_a * jax.nn.sigmoid(glu_b)).astype(jnp.bfloat16)
    prev_rows = shifted(gated_rows[tok_dev - (KW - 1) :], "sp", 1)
    padded = jnp.concatenate([prev_rows, gated_rows], axis=0)
    conv_sum = jnp.zeros((tok_dev, conv_local), jnp.float32)
    for tap_idx in range(KW):
        conv_sum = conv_sum + conv_taps[tap_idx] * padded[tap_idx : tap_idx + tok_dev].astype(
            jnp.float32
        )
    chan_total = conv_local * tp_count
    sums = jnp.concatenate([jnp.sum(conv_sum, axis=1), jnp.sum(conv_sum * conv_sum, axis=1)])
    sums = jnp.sum(sent_to_all(sums, "tp").reshape(tp_count, -1), axis=0)
    mean_val = (sums[:tok_dev] / chan_total)[:, None]
    mean_sq = (sums[tok_dev:] / chan_total)[:, None]
    conv_out = jax.nn.silu(
        (conv_sum - mean_val) * lax.rsqrt(mean_sq - mean_val * mean_val + 1e-05) * ln_gain
    ).astype(jnp.bfloat16)
    out_part = jnp.dot(conv_out, w_out_conv, preferred_element_type=jnp.float32)

    state = attend(where, both_q, (own, left, right, far), None, 0)
    for step in range(1, 5):
        if step < 4:
            new_up = sp_send(up if step < 3 else up[:1024], lambda z, x, c: (z + 1, x, c))
            new_down = sp_send(down if step < 3 else down[1024:], lambda z, x, c: (z - 1, x, c))
        state = attend(where, both_q, (up, down), state, step)
        if step < 4:
            up, down = new_up, new_down

    stats, acc = state
    half = 2 * heads
    swap = lambda z, x, c: (z, x, 1 - c)
    other_stats, other_acc = sp_send(stats[half:, :2], swap), sp_send(acc[half:], swap)
    m_a, l_a, m_b, l_b = stats[:half, 0], stats[:half, 1], other_stats[:, 0], other_stats[:, 1]
    m_all = jnp.maximum(m_a, m_b)
    w_a, w_b = jnp.exp2(m_a - m_all), jnp.exp2(m_b - m_all)
    l_all = l_a * w_a + l_b * w_b
    maps = (acc[:half] * w_a[:, None] + other_acc * w_b[:, None]) / l_all[:, None]
    maps = maps.reshape(heads, 2, 128, tok_dev)
    diff = maps[:, 0] - lam_head[:, None, None] * maps[:, 1]
    head_out = (
        diff
        * lax.rsqrt(jnp.mean(diff * diff, axis=1, keepdims=True) + 1e-06)
        * sub_gain[:, None]
    ).astype(jnp.bfloat16)
    attn_out = head_out.reshape(heads * 128, tok_dev).T
    log_sums = (m_all * LN2 + jnp.log(l_all)).reshape(heads, 2, tok_dev).transpose(1, 0, 2)

    out_part = out_part + jnp.dot(attn_out, w_out_attn, preferred_element_type=jnp.float32)
    out_part = lax.optimization_barrier(out_part.astype(jnp.bfloat16))
    blocks = lax.all_to_all(out_part.reshape(tp_count, -1, out_part.shape[1]), "tp", 0, 0, tiled=True)
    mixed = jnp.sum(blocks.astype(jnp.float32), axis=0).astype(jnp.bfloat16)
    return (mixed, log_sums)


def solution(mesh):
    return jax.shard_map(
        on_device,
        mesh=mesh,
        in_specs=(
            P(("sp", "tp"), None),
            P(),
            P(None, "tp"),
            P(None, "tp"),
            P(None, "tp"),
            P("tp"),
            P(None, "tp"),
            P(None, "tp"),
            P(None, "tp"),
            P("tp", None),
            P("tp", None),
            P("tp"),
            P(),
            P("tp", None),
            P("tp", None),
        ),
        out_specs=(P(("sp", "tp"), None), P(None, "tp", "sp")),
        check_vma=False,
    )
```

time: 387 us -> 156 us (0.40)
  the two profiles are of different devices: /device:TPU:34 before, /device:TPU:224 now
where the time goes in v1:
time: 156 us; the launch traced here: 155 us
  Pallas kernels  47.3 us (30%)
  starting transfers between devices  32.7 us (21%)
  waiting for transfers between devices  29.1 us (19%)
  local copies, waits for them, and re-layouts  16.7 us (11%)
  matrix products  14.7 us (9%)
  other arithmetic  13.7 us (9%)
    pallas_call x5, Pallas kernels, attend(): pl.pallas_call(body, out_shape=tuple((STATE(s) for s in shapes)), in_spec...  47.3 us
    ppermute x14, starting transfers between devices, sp_send(): return lax.ppermute(value, 'sp', sp_table(move))  18.3 us
    all_to_all x1, waiting for transfers between devices, on_device(): lax.all_to_all(out_part.reshape(tp_count, -1, out_part.shape[1]), 'tp', 0...  14.7 us
    all_to_all x2, waiting for transfers between devices, sent_to_all(): lax.all_to_all(jnp.broadcast_to(value[None], (count, *value.shape)), axis...  12.4 us
    all_to_all x2, starting transfers between devices, sent_to_all(): lax.all_to_all(jnp.broadcast_to(value[None], (count, *value.shape)), axis...  7.89 us
    unnamed x36, local copies, waits for them, and re-layouts  6.91 us
    all_to_all x1, starting transfers between devices, on_device(): lax.all_to_all(out_part.reshape(tp_count, -1, out_part.shape[1]), 'tp', 0...  4.57 us
    convert_element_type x2, other arithmetic, on_device(): query_t = (query_t * lax.rsqrt(jnp.mean(query_t * query_t, axis=1, keepdi...  3.89 us
  transfers between devices with their start and end apart: 18, of which 4 were waited for; matrix products, arithmetic and copies ran while one was open for 20% of the time, Pallas kernels for 30%

profile of v1, /device:TPU:224, one launch (start us, length us, event | category | flops | bytes accessed | tf_op | source)
XLA Modules:
  0.0 155.3 jit_solution(10860890985911207485)
XLA Ops:
  4.2 4.5 %all-to-all-start = ((bf16[4,64,2048]{2,1,0:T(8,128)(2,1)}), bf16[4,64,2048]{2,1,0:T(8,128)(2,1)}, u32[]{:S(2)}, u32[]{:S(2)}) async-start(bf16[4,64,2048]{2,1,0:T(8,128)(2,1)} %broadcast_in_dim.4), calls=%async_computation | async-start | bytes 2097152 | tf_op jit(solution)/shard_map/all_to_all | solution.py:38
  11.4 12.4 %all-to-all-done = bf16[4,64,2048]{2,1,0:T(8,128)(2,1)} async-done(((bf16[4,64,2048]{2,1,0:T(8,128)(2,1)}), bf16[4,64,2048]{2,1,0:T(8,128)(2,1)}, u32[]{:S(2)}, u32[]{:S(2)}) %all-to-all-start) | async-done | bytes 1048608 | tf_op jit(solution)/shard_map/all_to_all | solution.py:38
  32.2 1.8 %collective-permute-start.4 = (bf16[512,128]{1,0:T(8,128)(2,1)S(1)}, bf16[512,128]{1,0:T(8,128)(2,1)S(1)}, u32[]{:S(2)}, u32[]{:S(2)}) collective-permute-start(bf16[512,128]{1,0:T(8,128)(2,1)S(1)} %pad_maximum_fusion.2.own_ref), channel_id=1, source_target_pairs={{0,16},{4,20},{8,24},{12,28},{16,0},{20,4},{24,8},{28,12},{32,48},... | collective-permute-start | bytes 393224 | tf_op jit(solution)/shard_map/ppermute | solution.py:27
  34.0 2.7 %convolution_bitcast_fusion = f32[512,256]{0,1:T(8,128)} fusion(bf16[256,2048]{1,0:T(8,128)(2,1)} %bitcast.1, bf16[2048,512]{1,0:T(8,128)(2,1)S(1)} %copy-done.11), kind=kOutput, calls=%fused_computation.32 | convolution fusion | flops 536870912 | bytes 3670016 | tf_op jit(solution)/shard_map/dot_general | solution.py:237
  38.6 2.8 %fusion.3 = f32[256,512]{1,0:T(8,128)S(1)} fusion(bf16[256,2048]{1,0:T(8,128)(2,1)} %bitcast.1, bf16[2048,512]{1,0:T(8,128)(2,1)} %param.18), kind=kOutput, calls=%fused_computation.36 | convolution fusion | flops 537264128 | bytes 3670016 | tf_op jit(solution)/shard_map/dot_general | solution.py:252
  41.5 1.9 %fusion.4 = bf16[256,512]{1,0:T(8,128)(2,1)S(1)} fusion(f32[256,512]{1,0:T(8,128)S(1)} %fusion.3, bf16[256,2048]{1,0:T(8,128)(2,1)} %bitcast.1, bf16[2048,512]{1,0:T(8,128)(2,1)S(1)} %copy-done.5), kind=kOutput, calls=%fused_computation.37 | convolution fusion | flops 537133056 | bytes 3932160 | tf_op jit(solution)/shard_map/dot_general | solution.py:251
  45.5 2.0 %collective-permute-start.9 = (bf16[2048,128]{1,0:T(8,128)(2,1)}, bf16[2048,128]{1,0:T(8,128)(2,1)}, u32[]{:S(2)}, u32[]{:S(2)}) collective-permute-start(bf16[2048,128]{1,0:T(8,128)(2,1)} %constant_dynamic-update-slice_fusion), channel_id=1, source_target_pairs={{0,224},{4,228},{8,232},{12,236},{16,240},{20,244},{24,248},{28,25... | collective-permute-start | bytes 1572872 | tf_op jit(solution)/shard_map/ppermute | solution.py:27
  48.3 2.0 %copy.65 = f32[512,256]{0,1:T(8,128)} copy(f32[512,256]{1,0:T(8,128)} %bitcast.109) | data formatting | bytes 1048576 | tf_op jit(solution)/shard_map/mul | solution.py:241
  50.4 1.9 %collective-permute-start = (bf16[30,512]{1,0:T(8,128)(2,1)S(1)}, bf16[30,512]{1,0:T(8,128)(2,1)S(1)}, u32[]{:S(2)}, u32[]{:S(2)}) collective-permute-start(bf16[30,512]{1,0:T(8,128)(2,1)S(1)} %slice.308), channel_id=1, source_target_pairs={{0,4},{4,8},{8,12},{12,16},{16,20},{20,24},{24,28},{28,32},{32,36}... | collective-permute-start | bytes 92168 | tf_op jit(solution)/shard_map/ppermute | solution.py:33
  52.3 2.0 %multiply_convert_fusion = bf16[512,256]{0,1:T(8,128)(2,1)} fusion(f32[512,256]{0,1:T(8,128)} %convolution_bitcast_fusion, f32[512,256]{0,1:T(8,128)} %copy.65, f32[512]{0:T(512)S(1)} %bitcast.114), kind=kLoop, calls=%fused_computation.56 | loop fusion | flops 393216 | bytes 1312768 | tf_op jit(solution)/shard_map/convert_element_type | solution.py:244
  54.3 1.9 %multiply_convert_fusion.1 = bf16[8,64,256]{2,1,0:T(8,128)(2,1)} fusion(f32[8,64]{1,0:T(8,128)S(1)} %mul.604, f32[8,256]{1,0:T(8,128)S(1)} %add_rsqrt_fusion, f32[512,256]{1,0:T(8,128)} %copy-done.3), kind=kLoop, calls=%fused_computation.57 | loop fusion | flops 393216 | bytes 796672 | tf_op jit(solution)/shard_map/convert_element_type | solution.py:244
  59.2 2.7 %collective-permute-start.6 = (bf16[2048,128]{1,0:T(8,128)(2,1)S(1)}, bf16[2048,128]{1,0:T(8,128)(2,1)}, u32[]{:S(2)}, u32[]{:S(2)}) collective-permute-start(bf16[2048,128]{1,0:T(8,128)(2,1)S(1)} %collective-permute-done.5.a_ref), channel_id=1, source_target_pairs={{0,32},{4,36},{8,40},{12,44},{16,48},{20,52},{24,56},{28,60},{32,6... | collective-permute-start | bytes 1572872 | tf_op jit(solution)/shard_map/ppermute | solution.py:27
  61.9 3.3 %fusion.57 = (f32[256]{0:T(256)S(1)}, f32[256]{0:T(256)S(1)}, f32[256,512]{1,0:T(8,128)}) fusion(bf16[256,512]{1,0:T(8,128)(2,1)S(1)} %fusion.4, f32[512]{0:T(512)S(1)} %bitcast.125, bf16[30,512]{1,0:T(8,128)(2,1)S(1)} %collective-permute-done, f32[512]{0:T(512)S(1)} %bitcast.126, f32[512]{0:T(512)S(1)} %bitcast.128, f32[512]{0:T(512)S(1)} %bitcast.129, ...), kind=kLoop, calls=%fused_computation.146 | loop fusion | flops 24247808 | bytes 882688 | tf_op jit(solution)/shard_map/reduce_sum | solution.py:262
  65.9 3.4 %all-to-all-start.1 = ((f32[4,1,512]{2,1,0:T(1,128)}), f32[4,1,512]{2,1,0:T(1,128)S(1)}, u32[]{:S(2)}, u32[]{:S(2)}) async-start(f32[4,1,512]{2,1,0:T(1,128)} %broadcast_in_dim.5), calls=%async_computation.1 | async-start | bytes 16384 | tf_op jit(solution)/shard_map/all_to_all | solution.py:38
  71.4 7.2 %attend_0.1 = (f32[16,8,256]{2,1,0:T(8,128)S(1)}, f32[16,128,256]{2,1,0:T(8,128)S(1)}) custom-call(s32[3]{0:T(128)S(1)} %pad_add_fusion.where_ref, bf16[16,64,256]{2,1,0:T(8,128)(2,1)S(1)} %pad_maximum_fusion.q_in, bf16[512,128]{1,0:T(8,128)(2,1)S(1)} %pad_maximum_fusion.2.own_ref, bf16[512,128]{1,0:T(8,128)(2,1)S(1)} %collective-permute-done.2.left_ref, ...), custom_call_target="tpu_custom_call" | custom-call | flops 2147483648 | bytes 6291456 | tf_op jit(solution)/shard_map/attend_0/pallas_call | solution.py:171
  78.7 3.2 %collective-permute-start.7 = (bf16[2048,128]{1,0:T(8,128)(2,1)}, bf16[2048,128]{1,0:T(8,128)(2,1)S(1)}, u32[]{:S(2)}, u32[]{:S(2)}) collective-permute-start(bf16[2048,128]{1,0:T(8,128)(2,1)} %collective-permute-done.6.a_ref), channel_id=1, source_target_pairs={{0,32},{4,36},{8,40},{12,44},{16,48},{20,52},{24,56},{28,60},{32,6... | collective-permute-start | bytes 1572872 | tf_op jit(solution)/shard_map/ppermute | solution.py:27
  81.9 11.2 %attend_1.1 = (f32[16,8,256]{2,1,0:T(8,128)S(1)}, f32[16,128,256]{2,1,0:T(8,128)S(1)}) custom-call(s32[3]{0:T(128)S(1)} %pad_add_fusion.where_ref, bf16[16,64,256]{2,1,0:T(8,128)(2,1)S(1)} %pad_maximum_fusion.q_in, bf16[2048,128]{1,0:T(8,128)(2,1)S(1)} %collective-permute-done.5.a_ref, ...), custom_call_target="tpu_custom_call", output_to_operand_aliasing={{0}: (4, {}), {1}: (5, {})} | custom-call | flops 4294967296 | bytes 6291456 | tf_op jit(solution)/shard_map/attend_1/pallas_call | solution.py:171
  93.2 11.2 %attend_2.1 = (f32[16,8,256]{2,1,0:T(8,128)S(1)}, f32[16,128,256]{2,1,0:T(8,128)S(1)}) custom-call(s32[3]{0:T(128)S(1)} %pad_add_fusion.where_ref, bf16[16,64,256]{2,1,0:T(8,128)(2,1)S(1)} %pad_maximum_fusion.q_in, bf16[2048,128]{1,0:T(8,128)(2,1)} %collective-permute-done.6.a_ref, ...), custom_call_target="tpu_custom_call", output_to_operand_aliasing={{0}: (4, {}), {1}: (5, {})} | custom-call | flops 4294967296 | bytes 6291456 | tf_op jit(solution)/shard_map/attend_2/pallas_call | solution.py:171
  104.5 3.3 %collective-permute-start.8 = (bf16[1024,128]{1,0:T(8,128)(2,1)S(1)}, bf16[1024,128]{1,0:T(8,128)(2,1)S(1)}, u32[]{:S(2)}, u32[]{:S(2)}) collective-permute-start(bf16[1024,128]{1,0:T(8,128)(2,1)S(1)} %slice.369), channel_id=1, source_target_pairs={{0,32},{4,36},{8,40},{12,44},{16,48},{20,52},{24,56},{28,60},{32,6... | collective-permute-start | bytes 786440 | tf_op jit(solution)/shard_map/ppermute | solution.py:27
  107.8 10.9 %attend_3.1 = (f32[16,8,256]{2,1,0:T(8,128)S(1)}, f32[16,128,256]{2,1,0:T(8,128)S(1)}) custom-call(s32[3]{0:T(128)S(1)} %pad_add_fusion.where_ref, bf16[16,64,256]{2,1,0:T(8,128)(2,1)S(1)} %pad_maximum_fusion.q_in, bf16[2048,128]{1,0:T(8,128)(2,1)S(1)} %collective-permute-done.7.a_ref, ...), custom_call_target="tpu_custom_call", output_to_operand_aliasing={{0}: (4, {}), {1}: (5, {})} | custom-call | flops 4294967296 | bytes 6291456 | tf_op jit(solution)/shard_map/attend_3/pallas_call | solution.py:171
  118.8 6.7 %attend_4.1 = (f32[16,8,256]{2,1,0:T(8,128)S(1)}, f32[16,128,256]{2,1,0:T(8,128)S(1)}) custom-call(s32[3]{0:T(128)S(1)} %pad_add_fusion.where_ref, bf16[16,64,256]{2,1,0:T(8,128)(2,1)S(1)} %pad_maximum_fusion.q_in, bf16[1024,128]{1,0:T(8,128)(2,1)S(1)} %collective-permute-done.8.a_ref, ...), custom_call_target="tpu_custom_call", output_to_operand_aliasing={{0}: (4, {}), {1}: (5, {})} | custom-call | flops 2147483648 | bytes 6291456 | tf_op jit(solution)/shard_map/attend_4/pallas_call | solution.py:171
  128.7 2.0 %fusion.14 = f32[256,2048]{1,0:T(8,128)S(1)} fusion(bf16[512,2048]{1,0:T(8,128)(2,1)S(1)} %copy-done, f32[256,512]{1,0:T(8,128)} %get-tuple-element.31, f32[512]{0:T(512)S(1)} %copy-done.12, f32[256]{0:T(256)S(1)} %get-tuple-element.74, f32[256]{0:T(256)S(1)} %get-tuple-element.73), kind=kOutput, calls=%fused_computation.62 | convolution fusion | flops 537919488 | bytes 4722688 | tf_op jit(solution)/shard_map/dot_general | solution.py:269
  134.4 4.6 %all-to-all-start.2 = ((bf16[4,64,2048]{2,1,0:T(8,128)(2,1)}), bf16[4,64,2048]{2,1,0:T(8,128)(2,1)S(1)}, u32[]{:S(2)}, u32[]{:S(2)}) async-start(bf16[4,64,2048]{2,1,0:T(8,128)(2,1)} %bitcast.108), calls=%async_computation.2 | async-start | bytes 2097152 | tf_op jit(solution)/shard_map/all_to_all | solution.py:301
  139.7 14.7 %all-to-all-done.2 = bf16[4,64,2048]{2,1,0:T(8,128)(2,1)S(1)} async-done(((bf16[4,64,2048]{2,1,0:T(8,128)(2,1)}), bf16[4,64,2048]{2,1,0:T(8,128)(2,1)S(1)}, u32[]{:S(2)}, u32[]{:S(2)}) %all-to-all-start.2) | async-done | bytes 1048608 | tf_op jit(solution)/shard_map/all_to_all | solution.py:301
  (108 shorter events, 33.6 us)
Async XLA Ops:
  0.6 128.0 %copy-start = (bf16[512,2048]{1,0:T(8,128)(2,1)S(1)}, bf16[512,2048]{1,0:T(8,128)(2,1)}, u32[]{:S(2)}) copy-start(bf16[512,2048]{1,0:T(8,128)(2,1)} %param.28) | copy-start | bytes 6291460
  3.0 7.5 %copy-start.13 = (f32[1,128]{1,0:T(1,128)S(1)}, f32[1,128]{1,0:T(1,128)}, u32[]{:S(2)}) copy-start(f32[1,128]{1,0:T(1,128)} %param.25) | copy-start | bytes 1540
  3.0 8.2 %copy-start.8 = (f32[4,128]{1,0:T(4,128)S(1)}, f32[4,128]{1,0:T(4,128)}, u32[]{:S(2)}) copy-start(f32[4,128]{1,0:T(4,128)} %param.24) | copy-start | bytes 6148
  3.0 8.3 %copy-start.7 = (f32[31,512]{1,0:T(8,128)S(1)}, f32[31,512]{1,0:T(8,128)}, u32[]{:S(2)}) copy-start(f32[31,512]{1,0:T(8,128)} %param.19) | copy-start | bytes 190468
  4.2 19.7 %all-to-all-start = ((bf16[4,64,2048]{2,1,0:T(8,128)(2,1)}), bf16[4,64,2048]{2,1,0:T(8,128)(2,1)}, u32[]{:S(2)}, u32[]{:S(2)}) async-start(bf16[4,64,2048]{2,1,0:T(8,128)(2,1)} %broadcast_in_dim.4), calls=%async_computation | async-start | bytes 2097152 | tf_op jit(solution)/shard_map/all_to_all | solution.py:38
  8.6 17.8 %copy-start.6 = (bf16[2048,128]{1,0:T(8,128)(2,1)S(1)}, bf16[2048,128]{1,0:T(8,128)(2,1)}, u32[]{:S(2)}) copy-start(bf16[2048,128]{1,0:T(8,128)(2,1)} %param.23) | copy-start | bytes 1572868
  25.8 8.2 %copy-start.11 = (bf16[2048,512]{1,0:T(8,128)(2,1)S(1)}, bf16[2048,512]{1,0:T(8,128)(2,1)}, u32[]{:S(2)}) copy-start(bf16[2048,512]{1,0:T(8,128)(2,1)} %param.21) | copy-start | bytes 6291460
  28.8 14.6 %collective-permute-start.2 = (bf16[512,128]{1,0:T(8,128)(2,1)S(1)}, bf16[512,128]{1,0:T(8,128)(2,1)S(1)}, u32[]{:S(2)}, u32[]{:S(2)}) collective-permute-start(bf16[512,128]{1,0:T(8,128)(2,1)S(1)} %pad_maximum_fusion.2.own_ref), channel_id=1, source_target_pairs={{0,8},{4,12},{8,16},{12,20},{16,24},{20,28},{24,0},{28,4},{32,40},... | collective-permute-start | bytes 393224 | tf_op jit(solution)/shard_map/ppermute | solution.py:27
  30.4 13.7 %collective-permute-start.3 = (bf16[512,128]{1,0:T(8,128)(2,1)S(1)}, bf16[512,128]{1,0:T(8,128)(2,1)S(1)}, u32[]{:S(2)}, u32[]{:S(2)}) collective-permute-start(bf16[512,128]{1,0:T(8,128)(2,1)S(1)} %pad_maximum_fusion.2.own_ref), channel_id=1, source_target_pairs={{0,24},{4,28},{8,0},{12,4},{16,8},{20,12},{24,16},{28,20},{32,56},... | collective-permute-start | bytes 393224 | tf_op jit(solution)/shard_map/ppermute | solution.py:27
  32.2 12.6 %collective-permute-start.4 = (bf16[512,128]{1,0:T(8,128)(2,1)S(1)}, bf16[512,128]{1,0:T(8,128)(2,1)S(1)}, u32[]{:S(2)}, u32[]{:S(2)}) collective-permute-start(bf16[512,128]{1,0:T(8,128)(2,1)S(1)} %pad_maximum_fusion.2.own_ref), channel_id=1, source_target_pairs={{0,16},{4,20},{8,24},{12,28},{16,0},{20,4},{24,8},{28,12},{32,48},... | collective-permute-start | bytes 393224 | tf_op jit(solution)/shard_map/ppermute | solution.py:27
  45.5 13.8 %collective-permute-start.5 = (bf16[2048,128]{1,0:T(8,128)(2,1)}, bf16[2048,128]{1,0:T(8,128)(2,1)S(1)}, u32[]{:S(2)}, u32[]{:S(2)}) collective-permute-start(bf16[2048,128]{1,0:T(8,128)(2,1)} %constant_dynamic-update-slice_fusion), channel_id=1, source_target_pairs={{0,32},{4,36},{8,40},{12,44},{16,48},{20,52},{24,56},{28,60},{32,6... | collective-permute-start | bytes 1572872 | tf_op jit(solution)/shard_map/ppermute | solution.py:27
  45.5 13.2 %collective-permute-start.9 = (bf16[2048,128]{1,0:T(8,128)(2,1)}, bf16[2048,128]{1,0:T(8,128)(2,1)}, u32[]{:S(2)}, u32[]{:S(2)}) collective-permute-start(bf16[2048,128]{1,0:T(8,128)(2,1)} %constant_dynamic-update-slice_fusion), channel_id=1, source_target_pairs={{0,224},{4,228},{8,232},{12,236},{16,240},{20,244},{24,248},{28,25... | collective-permute-start | bytes 1572872 | tf_op jit(solution)/shard_map/ppermute | solution.py:27
  50.4 11.6 %collective-permute-start = (bf16[30,512]{1,0:T(8,128)(2,1)S(1)}, bf16[30,512]{1,0:T(8,128)(2,1)S(1)}, u32[]{:S(2)}, u32[]{:S(2)}) collective-permute-start(bf16[30,512]{1,0:T(8,128)(2,1)S(1)} %slice.308), channel_id=1, source_target_pairs={{0,4},{4,8},{8,12},{12,16},{16,20},{20,24},{24,28},{28,32},{32,36}... | collective-permute-start | bytes 92168 | tf_op jit(solution)/shard_map/ppermute | solution.py:33
  56.2 13.1 %collective-permute-start.1 = (bf16[512,256]{0,1:T(8,128)(2,1)}, bf16[512,256]{0,1:T(8,128)(2,1)}, u32[]{:S(2)}, u32[]{:S(2)}) collective-permute-start(bf16[512,256]{0,1:T(8,128)(2,1)} %multiply_convert_fusion), channel_id=1, source_target_pairs={{0,4},{4,0},{8,12},{12,8},{16,20},{20,16},{24,28},{28,24},{32,36},... | collective-permute-start | bytes 786440 | tf_op jit(solution)/shard_map/ppermute | solution.py:27
  58.7 19.9 %collective-permute-start.10 = (bf16[2048,128]{1,0:T(8,128)(2,1)}, bf16[2048,128]{1,0:T(8,128)(2,1)}, u32[]{:S(2)}, u32[]{:S(2)}) collective-permute-start(bf16[2048,128]{1,0:T(8,128)(2,1)} %collective-permute-done.9.b_ref), channel_id=1, source_target_pairs={{0,224},{4,228},{8,232},{12,236},{16,240},{20,244},{24,248},{28,25... | collective-permute-start | bytes 1572872 | tf_op jit(solution)/shard_map/ppermute | solution.py:27
  59.2 19.5 %collective-permute-start.6 = (bf16[2048,128]{1,0:T(8,128)(2,1)S(1)}, bf16[2048,128]{1,0:T(8,128)(2,1)}, u32[]{:S(2)}, u32[]{:S(2)}) collective-permute-start(bf16[2048,128]{1,0:T(8,128)(2,1)S(1)} %collective-permute-done.5.a_ref), channel_id=1, source_target_pairs={{0,32},{4,36},{8,40},{12,44},{16,48},{20,52},{24,56},{28,60},{32,6... | collective-permute-start | bytes 1572872 | tf_op jit(solution)/shard_map/ppermute | solution.py:27
  65.9 62.1 %all-to-all-start.1 = ((f32[4,1,512]{2,1,0:T(1,128)}), f32[4,1,512]{2,1,0:T(1,128)S(1)}, u32[]{:S(2)}, u32[]{:S(2)}) async-start(f32[4,1,512]{2,1,0:T(1,128)} %broadcast_in_dim.5), calls=%async_computation.1 | async-start | bytes 16384 | tf_op jit(solution)/shard_map/all_to_all | solution.py:38
  78.6 25.7 %collective-permute-start.11 = (bf16[2048,128]{1,0:T(8,128)(2,1)}, bf16[2048,128]{1,0:T(8,128)(2,1)S(1)}, u32[]{:S(2)}, u32[]{:S(2)}) collective-permute-start(bf16[2048,128]{1,0:T(8,128)(2,1)} %collective-permute-done.10.b_ref), channel_id=1, source_target_pairs={{0,224},{4,228},{8,232},{12,236},{16,240},{20,244},{24,248},{28,25... | collective-permute-start | bytes 1572872 | tf_op jit(solution)/shard_map/ppermute | solution.py:27
  78.7 25.8 %collective-permute-start.7 = (bf16[2048,128]{1,0:T(8,128)(2,1)}, bf16[2048,128]{1,0:T(8,128)(2,1)S(1)}, u32[]{:S(2)}, u32[]{:S(2)}) collective-permute-start(bf16[2048,128]{1,0:T(8,128)(2,1)} %collective-permute-done.6.a_ref), channel_id=1, source_target_pairs={{0,32},{4,36},{8,40},{12,44},{16,48},{20,52},{24,56},{28,60},{32,6... | collective-permute-start | bytes 1572872 | tf_op jit(solution)/shard_map/ppermute | solution.py:27
  104.4 14.4 %collective-permute-start.12 = (bf16[1024,128]{1,0:T(8,128)(2,1)S(1)}, bf16[1024,128]{1,0:T(8,128)(2,1)S(1)}, u32[]{:S(2)}, u32[]{:S(2)}) collective-permute-start(bf16[1024,128]{1,0:T(8,128)(2,1)S(1)} %slice.370), channel_id=1, source_target_pairs={{0,224},{4,228},{8,232},{12,236},{16,240},{20,244},{24,248},{28,25... | collective-permute-start | bytes 786440 | tf_op jit(solution)/shard_map/ppermute | solution.py:27
  104.5 14.3 %collective-permute-start.8 = (bf16[1024,128]{1,0:T(8,128)(2,1)S(1)}, bf16[1024,128]{1,0:T(8,128)(2,1)S(1)}, u32[]{:S(2)}, u32[]{:S(2)}) collective-permute-start(bf16[1024,128]{1,0:T(8,128)(2,1)S(1)} %slice.369), channel_id=1, source_target_pairs={{0,32},{4,36},{8,40},{12,44},{16,48},{20,52},{24,56},{28,60},{32,6... | collective-permute-start | bytes 786440 | tf_op jit(solution)/shard_map/ppermute | solution.py:27
  127.9 3.0 %collective-permute-start.14 = (f32[8,128,256]{2,1,0:T(8,128)}, f32[8,128,256]{2,1,0:T(8,128)S(1)}, u32[]{:S(2)}, u32[]{:S(2)}) collective-permute-start(f32[8,128,256]{2,1,0:T(8,128)} %slice.303), channel_id=1, source_target_pairs={{0,4},{4,0},{8,12},{12,8},{16,20},{20,16},{24,28},{28,24},{32,36},... | collective-permute-start | bytes 3145736 | tf_op jit(solution)/shard_map/ppermute | solution.py:27
  128.1 2.8 %collective-permute-start.13 = (f32[8,2,256]{2,1,0:T(2,128)S(1)}, f32[8,2,256]{2,1,0:T(2,128)S(1)}, u32[]{:S(2)}, u32[]{:S(2)}) collective-permute-start(f32[8,2,256]{2,1,0:T(2,128)S(1)} %slice.301), channel_id=1, source_target_pairs={{0,4},{4,0},{8,12},{12,8},{16,20},{20,16},{24,28},{28,24},{32,36},... | collective-permute-start | bytes 49160 | tf_op jit(solution)/shard_map/ppermute | solution.py:27
  134.4 20.0 %all-to-all-start.2 = ((bf16[4,64,2048]{2,1,0:T(8,128)(2,1)}), bf16[4,64,2048]{2,1,0:T(8,128)(2,1)S(1)}, u32[]{:S(2)}, u32[]{:S(2)}) async-start(bf16[4,64,2048]{2,1,0:T(8,128)(2,1)} %bitcast.108), calls=%async_computation.2 | async-start | bytes 2097152 | tf_op jit(solution)/shard_map/all_to_all | solution.py:301
  (8 other events, 21.4 us)

commit v2 on v1

v2 whole, which is shorter than its diff:
```python
import functools

import jax
import jax.numpy as jnp
from jax import lax
from jax.experimental import pallas as pl
from jax.experimental.pallas import tpu as pltpu
from jax.sharding import PartitionSpec as P

KW = 31
NEG = -1e30
LOG2E = 1.4426950408889634
LN2 = 0.6931471805599453
UNROLL = 2


def sp_table(move):
    table = []
    for index in range(64):
        z, x, core = index // 8, (index // 2) % 4, index % 2
        nz, nx, nc = move(z, x, core)
        table.append((index, (nz % 8) * 8 + (nx % 4) * 2 + nc))
    return table


def sp_send(value, move):
    return lax.ppermute(value, "sp", sp_table(move))


def mirrored(slabs):
    return [(z * 8 + r, (7 - z) * 8 + r) for z in slabs for r in range(8)]


def shifted(value, axis, steps):
    count = lax.axis_size(axis)
    leading, last = (max(0, -steps), min(count, count - steps))
    return lax.ppermute(value, axis, [(source, source + steps) for source in range(leading, last)])


def sent_to_all(value, axis):
    count = lax.axis_size(axis)
    return lax.all_to_all(
        jnp.broadcast_to(value[None], (count, *value.shape)), axis, 0, 0, tiled=True
    )


def chunk_refs(pieces):
    return [(ref, row) for ref in pieces for row in range(0, ref.shape[0], 512)]


def slab_pass(chunks, q_ref, state, s_refs, bias_ref, lo, hi):
    def score(pair, which, at):
        ref, row = chunks[at]
        keys = ref[row : row + 256, :]
        s = jnp.dot(
            jnp.concatenate([keys, keys], axis=1),
            q_ref[2 * pair + which],
            preferred_element_type=jnp.float32,
        )
        if bias_ref is not None:
            s = s + bias_ref[which, at * 256 : at * 256 + 256, :]
        s_refs[which][at * 256 : at * 256 + 256, :] = s
        return jnp.max(s.reshape(32, 8, 256), axis=0)

    def both(pair, which, top, later):
        stats_ref, o_ref = state[which], state[2 + which]
        m_prev = stats_ref[pair, 0:1, :]
        m_new = jnp.maximum(m_prev, jnp.max(top, axis=0, keepdims=True))
        alpha = jnp.exp2(m_prev - m_new)
        total, out, next_top = None, None, None
        for at, (ref, row) in enumerate(chunks):
            part = score(later, 1 - which, at)
            next_top = part if next_top is None else jnp.maximum(next_top, part)
            p = jnp.exp2(s_refs[which][at * 256 : at * 256 + 256, :] - m_new)
            part = jnp.sum(p.reshape(32, 8, 256), axis=0)
            total = part if total is None else total + part
            vt = jnp.concatenate(
                [ref[row + 256 : row + 384, :], ref[row + 384 : row + 512, :]], axis=1
            )
            part = jnp.dot(vt, p.astype(jnp.bfloat16), preferred_element_type=jnp.float32)
            out = part if out is None else out + part
        stats_ref[pair, 0:1, :] = m_new
        l_new = stats_ref[pair, 1:2, :] * alpha + jnp.sum(total, axis=0, keepdims=True)
        stats_ref[pair, 1:2, :] = l_new
        o_ref[pair] = o_ref[pair] * alpha + out
        return next_top

    top = None
    for at in range(len(chunks)):
        part = score(lo, 0, at)
        top = part if top is None else jnp.maximum(top, part)

    def some(i, top):
        pair = lo + i
        top = both(pair, 0, top, pair)
        return both(pair, 1, top, jnp.minimum(pair + 1, hi - 1))

    lax.fori_loop(0, hi - lo, some, top)


def spread_queries(q_in, q_ref):
    scale = LOG2E * q_in.shape[1] ** (-0.5)
    zero = jnp.zeros((64, 256), jnp.bfloat16)
    for unit in range(q_in.shape[0]):
        scaled = q_in[unit].astype(jnp.float32) * scale
        high = scaled.astype(jnp.bfloat16)
        low = (scaled - high.astype(jnp.float32)).astype(jnp.bfloat16)
        at = 64 * (unit // 2 % 2)
        for first, part in ((0, high), (128, low)):
            q_ref[unit, first + at : first + at + 64, :] = part
            q_ref[unit, first + 64 - at : first + 128 - at, :] = zero


def work_ends(z):
    moved = jnp.where((z == 0) | (z == 7), 2, jnp.where((z == 3) | (z == 4), 0, 1))
    own_end = jnp.where(z >= 4, 8 - 2 * moved, 8)
    guest_end = jnp.where(z < 4, 8 + 2 * moved, 8)
    return own_end, guest_end


def fill_bias(where_ref, bias_ref):
    x, core = where_ref[1], where_ref[2]
    key_at = lax.broadcasted_iota(jnp.int32, (256, 256), 0)
    query_at = lax.broadcasted_iota(jnp.int32, (256, 256), 1)
    bias_ref[0, 0:256, :] = jnp.where(key_at <= query_at, 0.0, NEG)
    bias_ref[1, 0:256, :] = jnp.full((256, 256), jnp.where(core == 0, 0.0, NEG), jnp.float32)
    for at, step in ((1, 3), (2, 1), (3, 2)):
        seen = jnp.where(lax.rem(x + step, 4) < x, 0.0, NEG)
        for which in range(2):
            bias_ref[which, at * 256 : at * 256 + 256, :] = jnp.full((256, 256), seen, jnp.float32)


def first_kernel(where_ref, q_in, own_ref, left_ref, right_ref, far_ref, *rest):
    state, (q_ref, s_a, s_b, bias_ref) = rest[:4], rest[4:]
    spread_queries(q_in, q_ref)
    for stats_ref, o_ref in zip(state[:2], state[2:]):
        stats_ref[...] = jnp.zeros_like(stats_ref)
        for pair in range(stats_ref.shape[0]):
            stats_ref[pair, 0:1, :] = jnp.full((1, 256), NEG, jnp.float32)
        o_ref[...] = jnp.zeros_like(o_ref)
    fill_bias(where_ref, bias_ref)
    own_end, guest_end = work_ends(where_ref[0])
    chunks = chunk_refs((own_ref, left_ref, right_ref, far_ref))
    slab_pass(chunks, q_ref, state, (s_a, s_b), bias_ref, 0, own_end)

    @pl.when(guest_end > 8)
    def _():
        slab_pass(chunks, q_ref, state, (s_a, s_b), None, 8, guest_end)


def slab_kernel(step, where_ref, q_in, a_ref, b_ref, *rest):
    state, (q_ref, s_a, s_b, bias_ref) = rest[4:8], rest[8:]
    for before, after in zip(rest[:4], state):
        after[...] = before[...]
    z = where_ref[0]
    spread_queries(q_in, q_ref)
    own_end, guest_end = work_ends(z)

    def go(slab, masked, *pieces):
        chunks = chunk_refs(pieces)
        own_seen, guest_seen = slab < z, (slab < 7 - z) & (z < 4)
        lo = jnp.where(own_seen, 0, 8)
        hi = jnp.where(guest_seen, guest_end, jnp.where(own_seen, own_end, 8))

        @pl.when(hi > lo)
        def _():
            slab_pass(chunks, q_ref, state, (s_a, s_b), None, lo, hi)

        if masked:

            @pl.when((slab == 7 - z) & (guest_end > 8))
            def _():
                fill_bias(where_ref, bias_ref)
                slab_pass(chunks, q_ref, state, (s_a, s_b), bias_ref, 8, guest_end)

    below, above = lax.rem(z + 8 - step, 8), lax.rem(z + step, 8)
    if step == 4:
        go(above, False, a_ref, b_ref)
    else:
        go(below, step in (1, 3), a_ref)
        go(above, step == 3, b_ref)


VMEM_SPEC = pl.BlockSpec(memory_space=pltpu.VMEM)
SMEM_SPEC = pl.BlockSpec(memory_space=pltpu.SMEM)


def plain_kernel(body, name, args, out_shape, scratch=(), aliases={}, flops=1 << 28, smem=1):
    return pl.pallas_call(
        body,
        out_shape=out_shape,
        in_specs=[SMEM_SPEC] * smem + [VMEM_SPEC] * (len(args) - smem),
        out_specs=jax.tree.map(lambda _: VMEM_SPEC, out_shape),
        scratch_shapes=scratch,
        input_output_aliases=aliases,
        compiler_params=pltpu.CompilerParams(vmem_limit_bytes=24 << 20),
        cost_estimate=pl.CostEstimate(flops=flops, bytes_accessed=2 << 20, transcendentals=0),
        name=name,
    )(*args)


def attend(where, q, pieces, state, step):
    units = q.shape[0]
    shapes = [(units // 2, 8, 256)] * 2 + [(units // 2, 128, 256)] * 2
    scratch = [
        pltpu.VMEM((units, 256, 256), jnp.bfloat16),
        pltpu.VMEM((1024, 256), jnp.float32),
        pltpu.VMEM((1024, 256), jnp.float32),
        pltpu.VMEM((2, 1024, 256), jnp.float32),
    ]
    if step == 0:
        body, args, aliases, keys = first_kernel, (where, q, *pieces), {}, 1024
    else:
        body, args = functools.partial(slab_kernel, step), (where, q, *pieces, *state)
        aliases = {4 + k: k for k in range(4)} if step < 4 else {}
        keys = sum(p.shape[0] for p in pieces) // 2
    kind = jax.ShapeDtypeStruct if step == 4 else pltpu.VMEM
    out_shape = tuple(kind(s, jnp.float32) for s in shapes)
    flops = keys * 256 * units * 256
    return plain_kernel(body, f"attend_{step}", args, out_shape, scratch, aliases, flops)


def front_kernel(where_ref, own_ref, left_ref, right_ref, far_ref, gain_ref, wk_ref, wv_ref, key_gain_ref, normed_ref, kv_ref):
    t = where_ref[3]
    for ref, step in ((own_ref, 0), (left_ref, 3), (right_ref, 1), (far_ref, 2)):
        row = pl.multiple_of(lax.rem(t + step, 4) * 64, 64)
        rows = ref[...].astype(jnp.float32)
        mean = jnp.mean(rows * rows, axis=1, keepdims=True)
        normed_ref[pl.ds(row, 64), :] = (rows * lax.rsqrt(mean + 1e-06) * gain_ref[...]).astype(
            jnp.bfloat16
        )
    normed = normed_ref[...]
    keys = jnp.dot(normed, wk_ref[...], preferred_element_type=jnp.float32)
    first = lax.broadcasted_iota(jnp.int32, keys.shape, 1) < 64
    square = keys * keys
    mean_a = jnp.sum(jnp.where(first, square, 0.0), axis=1, keepdims=True)
    mean_b = jnp.sum(jnp.where(first, 0.0, square), axis=1, keepdims=True)
    scale = jnp.where(
        first, lax.rsqrt(mean_a * (1 / 64) + 1e-06), lax.rsqrt(mean_b * (1 / 64) + 1e-06)
    )
    kv_ref[0:256, :] = (keys * scale * key_gain_ref[...]).astype(jnp.bfloat16)
    values = jnp.dot(normed, wv_ref[...], preferred_element_type=jnp.float32)
    for half in range(2):
        turned = values[half * 128 : half * 128 + 128, :].T
        kv_ref[256 + half * 128 : 384 + half * 128, :] = turned.astype(jnp.bfloat16)


def query_kernel(normed_ref, wq_ref, gain_ref, q_ref):
    normed = normed_ref[...]
    for part in range(wq_ref.shape[1] // 256):
        got = jnp.dot(
            normed, wq_ref[:, part * 256 : part * 256 + 256], preferred_element_type=jnp.float32
        )
        turned = got.T
        for k in range(4):
            at = part * 256 + k * 64
            q = turned[k * 64 : k * 64 + 64, :]
            mean = jnp.mean(q * q, axis=0, keepdims=True)
            q = q * lax.rsqrt(mean + 1e-06) * gain_ref[at : at + 64, :]
            q_ref[at : at + 64, :] = q.astype(jnp.bfloat16)


def finish_kernel(lam_ref, gain_ref, stats_a, acc_a, stats_b, acc_b, head_ref, log_ref):
    for head in range(head_ref.shape[0]):
        maps = []
        for half in range(2):
            pair = 2 * head + half
            m_a, m_b = stats_a[pair, 0:1, :], stats_b[pair, 0:1, :]
            m_all = jnp.maximum(m_a, m_b)
            w_a, w_b = jnp.exp2(m_a - m_all), jnp.exp2(m_b - m_all)
            l_all = stats_a[pair, 1:2, :] * w_a + stats_b[pair, 1:2, :] * w_b
            log_ref[pair, 0:1, :] = m_all * LN2 + jnp.log(l_all)
            maps.append((acc_a[pair] * w_a + acc_b[pair] * w_b) * (1.0 / l_all))
        diff = maps[0] - lam_ref[head] * maps[1]
        mean = jnp.mean(diff * diff, axis=0, keepdims=True)
        head_ref[head] = (diff * lax.rsqrt(mean + 1e-06) * gain_ref[...]).astype(jnp.bfloat16)


def on_device(
    tokens,
    norm_gain,
    w_glu_a,
    w_glu_b,
    conv_taps,
    ln_gain,
    w_query,
    w_key,
    w_value,
    query_gain,
    key_gain,
    lam_head,
    sub_gain,
    w_out_conv,
    w_out_attn,
):
    tp_count = lax.axis_size("tp")
    tok_dev = tokens.shape[0] * tp_count
    conv_local = w_glu_a.shape[1]
    heads = lam_head.shape[0]
    head_dim = key_gain.shape[1] // 2
    sp = lax.axis_index("sp")
    where = jnp.stack([sp // 8, (sp // 2) % 4, sp % 2, lax.axis_index("tp")]).astype(jnp.int32)

    rows_of = [
        lax.ppermute(tokens, "tp", [(t, (t + step) % 4) for t in range(4)]) for step in (2, 1, 3)
    ]
    normed_shape = jax.ShapeDtypeStruct((tok_dev, tokens.shape[1]), jnp.bfloat16)
    rows_block, own = plain_kernel(
        front_kernel,
        "front",
        (
            where,
            tokens,
            rows_of[1],
            rows_of[2],
            rows_of[0],
            norm_gain[None],
            w_key,
            w_value,
            key_gain,
        ),
        (normed_shape, jax.ShapeDtypeStruct((512, 128), jnp.bfloat16)),
    )

    query_t = plain_kernel(
        query_kernel,
        "queries",
        (rows_block, w_query, query_gain.reshape(-1, 1)),
        jax.ShapeDtypeStruct((w_query.shape[1], tok_dev), jnp.bfloat16),
        smem=0,
    )
    swap = lambda z, x, c: (z, x, 1 - c)
    query_t = query_t.reshape(heads, 2 * head_dim, tok_dev)
    given = jnp.stack([query_t[3], query_t[2]])
    guest = lax.ppermute(given, "sp", mirrored((7, 6, 5)))
    partner_q = sp_send(query_t, swap)
    left = sp_send(own, lambda z, x, c: (z, x + 1, c))
    right = sp_send(own, lambda z, x, c: (z, x - 1, c))
    far = sp_send(own, lambda z, x, c: (z, x + 2, c))
    guest_early, rows_block = lax.optimization_barrier((guest, rows_block))
    glu_a = jnp.dot(rows_block, w_glu_a, preferred_element_type=jnp.float32)
    glu_b = jnp.dot(rows_block, w_glu_b, preferred_element_type=jnp.float32)
    gated_rows = (glu_a * jax.nn.sigmoid(glu_b)).astype(jnp.bfloat16)
    prev_rows = shifted(gated_rows[tok_dev - (KW - 1) :], "sp", 1)
    partner_guest = sp_send(guest_early, swap)
    mine = jnp.concatenate([query_t, guest_early], axis=0).reshape(-1, head_dim, tok_dev)
    other = jnp.concatenate([partner_q, partner_guest], axis=0).reshape(-1, head_dim, tok_dev)
    both_q = jnp.stack([mine, other], axis=1).reshape(-1, head_dim, tok_dev)
    slab = jnp.concatenate([own, left, right, far], axis=0)

    slab, gated_rows = lax.optimization_barrier((slab, gated_rows))
    up = sp_send(slab, lambda z, x, c: (z + 1, x, c))
    down = sp_send(slab, lambda z, x, c: (z - 1, x, c))

    padded = jnp.concatenate([prev_rows, gated_rows], axis=0)
    conv_sum = jnp.zeros((tok_dev, conv_local), jnp.float32)
    for tap_idx in range(KW):
        conv_sum = conv_sum + conv_taps[tap_idx] * padded[tap_idx : tap_idx + tok_dev].astype(
            jnp.float32
        )
    chan_total = conv_local * tp_count
    sums = jnp.concatenate([jnp.sum(conv_sum, axis=1), jnp.sum(conv_sum * conv_sum, axis=1)])
    where_0, sums = lax.optimization_barrier((where, sums))
    sums = jnp.sum(sent_to_all(sums, "tp").reshape(tp_count, -1), axis=0)
    mean_val = (sums[:tok_dev] / chan_total)[:, None]
    mean_sq = (sums[tok_dev:] / chan_total)[:, None]
    conv_out = jax.nn.silu(
        (conv_sum - mean_val) * lax.rsqrt(mean_sq - mean_val * mean_val + 1e-05) * ln_gain
    ).astype(jnp.bfloat16)
    out_part = jnp.dot(conv_out, w_out_conv, preferred_element_type=jnp.float32)

    where_2, out_part = lax.optimization_barrier((where, out_part))

    state = attend(where_0, both_q, (own, left, right, far), None, 0)
    for step in range(1, 5):
        up, down, first = lax.optimization_barrier((up, down, state[0]))
        state = (first, *state[1:])
        if step < 4:
            new_up = sp_send(up if step < 3 else up[:1024], lambda z, x, c: (z + 1, x, c))
            new_down = sp_send(down if step < 3 else down[1024:], lambda z, x, c: (z - 1, x, c))
        state = attend(where if step == 1 else where_2, both_q, (up, down), state, step)
        if step < 4:
            up, down = new_up, new_down

    other_stats, other_acc = sp_send(state[1], swap), sp_send(state[3], swap)
    lam_all = jnp.concatenate([lam_head, lam_head[3:], lam_head[2:3]])
    pairs = state[0].shape[0]
    head_out, logs = plain_kernel(
        finish_kernel,
        "finish",
        (lam_all, sub_gain[:, None], state[0], state[2], other_stats, other_acc),
        (
            jax.ShapeDtypeStruct((pairs // 2, 128, tok_dev), jnp.bfloat16),
            jax.ShapeDtypeStruct((pairs, 8, tok_dev), jnp.float32),
        ),
    )
    logs = logs[:, 0].reshape(-1, 2, tok_dev)
    back_out = lax.ppermute(head_out[heads:], "sp", mirrored((0, 1, 2)))
    back_logs = lax.ppermute(logs[heads:], "sp", mirrored((0, 1, 2)))
    z = where[0]

    def with_guests(mine, back):
        third = jnp.where(z == 7, back[1], mine[2])
        fourth = jnp.where(z >= 5, back[0], mine[3])
        return jnp.concatenate([mine[:2], third[None], fourth[None]], axis=0)

    attn_t = with_guests(head_out, back_out).reshape(heads * 128, tok_dev)
    log_sums = with_guests(logs, back_logs).transpose(1, 0, 2)

    out_part = out_part + lax.dot_general(
        attn_t, w_out_attn, (((0,), (0,)), ((), ())), preferred_element_type=jnp.float32
    )
    out_part = lax.optimization_barrier(out_part.astype(jnp.bfloat16))
    blocks = lax.all_to_all(out_part.reshape(tp_count, -1, out_part.shape[1]), "tp", 0, 0, tiled=True)
    mixed = jnp.sum(blocks.astype(jnp.float32), axis=0).astype(jnp.bfloat16)
    return (mixed, log_sums)


def solution(mesh):
    return jax.shard_map(
        on_device,
        mesh=mesh,
        in_specs=(
            P(("sp", "tp"), None),
            P(),
            P(None, "tp"),
            P(None, "tp"),
            P(None, "tp"),
            P("tp"),
            P(None, "tp"),
            P(None, "tp"),
            P(None, "tp"),
            P("tp", None),
            P("tp", None),
            P("tp"),
            P(),
            P("tp", None),
            P("tp", None),
        ),
        out_specs=(P(("sp", "tp"), None), P(None, "tp", "sp")),
        check_vma=False,
    )
```

time: 156 us -> 161 us (1.032)
  the two profiles are of different devices: /device:TPU:224 before, /device:TPU:34 now
where the time goes in v2:
time: 161 us; the launch traced here: 160 us
  starting transfers between devices  58.9 us (37%)
  Pallas kernels  37.4 us (23%)
  waiting for transfers between devices  33.1 us (21%)
  local copies, waits for them, and re-layouts  11.5 us (7%)
  other arithmetic  10.5 us (7%)
  matrix products  7.62 us (5%)
    pallas_call x8, Pallas kernels, plain_kernel(): pl.pallas_call(body, out_shape=out_shape, in_specs=[SMEM_SPEC] * smem + [...  37.4 us
    ppermute x15, starting transfers between devices, sp_send(): return lax.ppermute(value, 'sp', sp_table(move))  19.4 us
    ppermute x1, starting transfers between devices, on_device(): back_out = lax.ppermute(head_out[heads:], 'sp', mirrored((0, 1, 2)))  15.8 us
    ppermute x3, waiting for transfers between devices, on_device(): lax.ppermute(tokens, 'tp', [(t, (t + step) % 4) for t in range(4)])  9.1 us
    ppermute x1, starting transfers between devices, on_device(): back_logs = lax.ppermute(logs[heads:], 'sp', mirrored((0, 1, 2)))  7.39 us
    unnamed x30, local copies, waits for them, and re-layouts  7 us
    ppermute x15, waiting for transfers between devices, sp_send(): return lax.ppermute(value, 'sp', sp_table(move))  6.54 us
    all_to_all x1, waiting for transfers between devices, on_device(): lax.all_to_all(out_part.reshape(tp_count, -1, out_part.shape[1]), 'tp', 0...  5.49 us
  transfers between devices with their start and end apart: 24, of which 11 were waited for; matrix products, arithmetic and copies ran while one was open for 10% of the time, Pallas kernels for 18%

profile of v2, /device:TPU:34, one launch (start us, length us, event | category | flops | bytes accessed | tf_op | source)
XLA Modules:
  0.0 159.9 jit_solution(9591192943035046909)
XLA Ops:
  7.9 2.3 %collective-permute-done.left_ref = bf16[64,2048]{1,0:T(8,128)(2,1)S(1)} collective-permute-done((bf16[64,2048]{1,0:T(8,128)(2,1)}, bf16[64,2048]{1,0:T(8,128)(2,1)S(1)}, u32[]{:S(2)}, u32[]{:S(2)}) %collective-permute-start) | collective-permute-done | bytes 262176 | tf_op jit(solution)/shard_map/ppermute | solution.py:305
  10.3 5.1 %collective-permute-done.1.right_ref = bf16[64,2048]{1,0:T(8,128)(2,1)S(1)} collective-permute-done((bf16[64,2048]{1,0:T(8,128)(2,1)}, bf16[64,2048]{1,0:T(8,128)(2,1)S(1)}, u32[]{:S(2)}, u32[]{:S(2)}) %collective-permute-start.1) | collective-permute-done | bytes 262176 | tf_op jit(solution)/shard_map/ppermute | solution.py:305
  28.6 2.1 %collective-permute-start.7 = (bf16[512,128]{1,0:T(8,128)(2,1)S(1)}, bf16[512,128]{1,0:T(8,128)(2,1)S(1)}, u32[]{:S(2)}, u32[]{:S(2)}) collective-permute-start(bf16[512,128]{1,0:T(8,128)(2,1)S(1)} %get-tuple-element.48.own_ref), channel_id=1, source_target_pairs={{0,16},{4,20},{8,24},{12,28},{16,0},{20,4},{24,8},{28,12},{32,48},... | collective-permute-start | bytes 393224 | tf_op jit(solution)/shard_map/ppermute | solution.py:27
  30.7 3.5 %collective-permute-done.3 = bf16[2,128,256]{2,1,0:T(8,128)(2,1)} collective-permute-done((bf16[2,128,256]{2,1,0:T(8,128)(2,1)S(1)}, bf16[2,128,256]{2,1,0:T(8,128)(2,1)}, u32[]{:S(2)}, u32[]{:S(2)}) %collective-permute-start.3) | collective-permute-done | bytes 131104 | tf_op jit(solution)/shard_map/ppermute | solution.py:335
  42.5 3.3 %fusion.40 = (f32[256]{0:T(256)S(1)}, f32[256]{0:T(256)S(1)}, f32[256,512]{1,0:T(8,128)}) fusion(bf16[256,512]{1,0:T(8,128)(2,1)S(1)} %fusion.4, f32[512]{0:T(512)S(1)} %bitcast.101, bf16[30,512]{1,0:T(8,128)(2,1)S(1)} %collective-permute-done.4, f32[512]{0:T(512)S(1)} %bitcast.102, f32[512]{0:T(512)S(1)} %bitcast.73, f32[512]{0:T(512)S(1)} %bitcast.74, ...), kind=kLoop, calls=%fused_computation.104 | loop fusion | flops 24247808 | bytes 882688 | tf_op jit(solution)/shard_map/reduce_sum | solution.py:362
  46.5 3.4 %all-to-all-start = ((f32[4,1,512]{2,1,0:T(1,128)}), f32[4,1,512]{2,1,0:T(1,128)S(1)}, u32[]{:S(2)}, u32[]{:S(2)}) async-start(f32[4,1,512]{2,1,0:T(1,128)} %broadcast_in_dim.7), calls=%async_computation | async-start | bytes 16384 | tf_op jit(solution)/shard_map/all_to_all | solution.py:42
  50.8 4.2 %all-to-all-done = f32[4,1,512]{2,1,0:T(1,128)S(1)} async-done(((f32[4,1,512]{2,1,0:T(1,128)}), f32[4,1,512]{2,1,0:T(1,128)S(1)}, u32[]{:S(2)}, u32[]{:S(2)}) %all-to-all-start) | async-done | bytes 8224 | tf_op jit(solution)/shard_map/all_to_all | solution.py:42
  56.1 9.5 %attend_0.1 = (f32[12,8,256]{2,1,0:T(8,128)S(1)}, f32[12,8,256]{2,1,0:T(8,128)S(1)}, f32[12,128,256]{2,1,0:T(8,128)S(1)}, f32[12,128,256]{2,1,0:T(8,128)S(1)}) custom-call(s32[4]{0:T(128)S(1)} %pad_add_fusion.where_ref, bf16[24,64,256]{2,1,0:T(8,128)(2,1)S(1)} %bitcast.63, bf16[512,128]{1,0:T(8,128)(2,1)S(1)} %get-tuple-element.48.own_ref, ...), custom_call_target="tpu_custom_call" | custom-call | flops 1610612736 | bytes 2097152 | tf_op jit(solution)/shard_map/attend_0/pallas_call | solution.py:189
  66.5 3.7 %collective-permute-start.13 = (bf16[2048,128]{1,0:T(8,128)(2,1)}, bf16[2048,128]{1,0:T(8,128)(2,1)S(1)}, u32[]{:S(2)}, u32[]{:S(2)}) collective-permute-start(bf16[2048,128]{1,0:T(8,128)(2,1)} %collective-permute-done.11.b_ref), channel_id=1, source_target_pairs={{0,224},{4,228},{8,232},{12,236},{16,240},{20,244},{24,248},{28,25... | collective-permute-start | bytes 1572872 | tf_op jit(solution)/shard_map/ppermute | solution.py:27
  70.2 11.3 %attend_1.1 = (f32[12,8,256]{2,1,0:T(8,128)S(1)}, f32[12,8,256]{2,1,0:T(8,128)S(1)}, f32[12,128,256]{2,1,0:T(8,128)S(1)}, f32[12,128,256]{2,1,0:T(8,128)S(1)}) custom-call(s32[4]{0:T(128)S(1)} %pad_add_fusion.where_ref, bf16[24,64,256]{2,1,0:T(8,128)(2,1)S(1)} %bitcast.64, ...), custom_call_target="tpu_custom_call", output_to_operand_aliasing={{0}: (4, {}), {1}: (5, {}), {2}: (6, {}), {3}: (7, {})} | custom-call | flops 3221225472 | bytes 2097152 | tf_op jit(solution)/shard_map/attend_1/pallas_call | solution.py:189
  81.6 2.7 %collective-permute-start.15 = (bf16[2048,128]{1,0:T(8,128)(2,1)S(1)}, bf16[2048,128]{1,0:T(8,128)(2,1)S(1)}, u32[]{:S(2)}, u32[]{:S(2)}) collective-permute-start(bf16[2048,128]{1,0:T(8,128)(2,1)S(1)} %collective-permute-done.13.b_ref), channel_id=1, source_target_pairs={{0,224},{4,228},{8,232},{12,236},{16,240},{20,244},{24,248},{28,25... | collective-permute-start | bytes 1572872 | tf_op jit(solution)/shard_map/ppermute | solution.py:27
  84.3 2.2 %fusion.5 = f32[256,2048]{1,0:T(8,128)} fusion(bf16[512,2048]{1,0:T(8,128)(2,1)S(1)} %copy-done, f32[256,512]{1,0:T(8,128)S(1)} %copy-done.10, f32[512]{0:T(512)S(1)} %copy-done.14, f32[256]{0:T(256)S(1)} %get-tuple-element.135, f32[256]{0:T(256)S(1)} %get-tuple-element.134), kind=kOutput, calls=%fused_computation.44 | convolution fusion | flops 537919488 | bytes 4722688 | tf_op jit(solution)/shard_map/dot_general | solution.py:370
  86.5 3.1 %attend_2.1 = (f32[12,8,256]{2,1,0:T(8,128)S(1)}, f32[12,8,256]{2,1,0:T(8,128)S(1)}, f32[12,128,256]{2,1,0:T(8,128)S(1)}, f32[12,128,256]{2,1,0:T(8,128)S(1)}) custom-call(s32[4]{0:T(128)S(1)} %pad_add_fusion.where_ref, bf16[24,64,256]{2,1,0:T(8,128)(2,1)S(1)} %bitcast.65, ...), custom_call_target="tpu_custom_call", output_to_operand_aliasing={{0}: (4, {}), {1}: (5, {}), {2}: (6, {}), {3}: (7, {})} | custom-call | flops 3221225472 | bytes 2097152 | tf_op jit(solution)/shard_map/attend_2/pallas_call | solution.py:189
  89.6 4.9 %collective-permute-done.14.a_ref = bf16[2048,128]{1,0:T(8,128)(2,1)S(1)} collective-permute-done((bf16[2048,128]{1,0:T(8,128)(2,1)S(1)}, bf16[2048,128]{1,0:T(8,128)(2,1)S(1)}, u32[]{:S(2)}, u32[]{:S(2)}) %collective-permute-start.14) | collective-permute-done | bytes 524320 | tf_op jit(solution)/shard_map/ppermute | solution.py:27
  94.5 2.2 %collective-permute-start.16 = (bf16[1024,128]{1,0:T(8,128)(2,1)S(1)}, bf16[1024,128]{1,0:T(8,128)(2,1)S(1)}, u32[]{:S(2)}, u32[]{:S(2)}) collective-permute-start(bf16[1024,128]{1,0:T(8,128)(2,1)S(1)} %slice.335), channel_id=1, source_target_pairs={{0,32},{4,36},{8,40},{12,44},{16,48},{20,52},{24,56},{28,60},{32,6... | collective-permute-start | bytes 786440 | tf_op jit(solution)/shard_map/ppermute | solution.py:27
  97.9 4.9 %attend_3.1 = (f32[12,8,256]{2,1,0:T(8,128)S(1)}, f32[12,8,256]{2,1,0:T(8,128)S(1)}, f32[12,128,256]{2,1,0:T(8,128)S(1)}, f32[12,128,256]{2,1,0:T(8,128)S(1)}) custom-call(s32[4]{0:T(128)S(1)} %pad_add_fusion.where_ref, bf16[24,64,256]{2,1,0:T(8,128)(2,1)S(1)} %bitcast.66, ...), custom_call_target="tpu_custom_call", output_to_operand_aliasing={{0}: (4, {}), {1}: (5, {}), {2}: (6, {}), {3}: (7, {})} | custom-call | flops 3221225472 | bytes 2097152 | tf_op jit(solution)/shard_map/attend_3/pallas_call | solution.py:189
  103.2 4.2 %attend_4.1 = (f32[12,8,256]{2,1,0:T(8,128)S(1)}, f32[12,8,256]{2,1,0:T(8,128)S(1)}, f32[12,128,256]{2,1,0:T(8,128)S(1)}, f32[12,128,256]{2,1,0:T(8,128)}) custom-call(s32[4]{0:T(128)S(1)} %pad_add_fusion.where_ref, bf16[24,64,256]{2,1,0:T(8,128)(2,1)S(1)} %bitcast.67, bf16[1024,128]{1,0:T(8,128)(2,1)S(1)} %collective-permute-done.16.a_ref, ...), custom_call_target="tpu_custom_call" | custom-call | flops 1610612736 | bytes 2097152 | tf_op jit(solution)/shard_map/attend_4/pallas_call | solution.py:189
  115.7 15.8 %collective-permute-start.20 = (bf16[2,128,256]{2,1,0:T(8,128)(2,1)S(1)}, bf16[2,128,256]{2,1,0:T(8,128)(2,1)S(1)}, u32[]{:S(2)}, u32[]{:S(2)}) collective-permute-start(bf16[2,128,256]{2,1,0:T(8,128)(2,1)S(1)} %get-tuple-element.98), channel_id=1, source_target_pairs={{0,224},{4,228},{8,232},{12,236},{16,240},{20,244},{24,248},{28,25... | collective-permute-start | bytes 393224 | tf_op jit(solution)/shard_map/ppermute | solution.py:398
  131.6 3.0 %collective-permute-done.20 = bf16[2,128,256]{2,1,0:T(8,128)(2,1)S(1)} collective-permute-done((bf16[2,128,256]{2,1,0:T(8,128)(2,1)S(1)}, bf16[2,128,256]{2,1,0:T(8,128)(2,1)S(1)}, u32[]{:S(2)}, u32[]{:S(2)}) %collective-permute-start.20) | collective-permute-done | bytes 131104 | tf_op jit(solution)/shard_map/ppermute | solution.py:398
  134.7 3.9 %fusion = bf16[256,2048]{1,0:T(8,128)(2,1)} fusion(f32[256,2048]{1,0:T(8,128)} %fusion.5, bf16[512,256]{1,0:T(8,128)(2,1)S(1)} %bitcast.71, bf16[512,2048]{1,0:T(8,128)(2,1)} %param.29), kind=kOutput, calls=%fused_computation.30 | convolution fusion | flops 537919488 | bytes 5505024 | tf_op jit(solution)/shard_map/dot_general | solution.py:410
  138.6 4.3 %all-to-all-start.1 = ((bf16[4,64,2048]{2,1,0:T(8,128)(2,1)}), bf16[4,64,2048]{2,1,0:T(8,128)(2,1)}, u32[]{:S(2)}, u32[]{:S(2)}) async-start(bf16[4,64,2048]{2,1,0:T(8,128)(2,1)} %bitcast.45), calls=%async_computation.1 | async-start | bytes 2097152 | tf_op jit(solution)/shard_map/all_to_all | solution.py:414
  142.9 7.4 %collective-permute-start.21 = (f32[2,2,256]{2,0,1:T(2,128)S(1)}, f32[2,2,256]{2,0,1:T(2,128)S(1)}, u32[]{:S(2)}, u32[]{:S(2)}) collective-permute-start(f32[2,2,256]{2,0,1:T(2,128)S(1)} %copy.42), channel_id=1, source_target_pairs={{0,224},{4,228},{8,232},{12,236},{16,240},{20,244},{24,248},{28,25... | collective-permute-start | bytes 12296 | tf_op jit(solution)/shard_map/ppermute | solution.py:399
  152.2 5.5 %all-to-all-done.1 = bf16[4,64,2048]{2,1,0:T(8,128)(2,1)} async-done(((bf16[4,64,2048]{2,1,0:T(8,128)(2,1)}), bf16[4,64,2048]{2,1,0:T(8,128)(2,1)}, u32[]{:S(2)}, u32[]{:S(2)}) %all-to-all-start.1) | async-done | bytes 1048608 | tf_op jit(solution)/shard_map/all_to_all | solution.py:414
  157.7 2.2 %reduce_sum.42 = bf16[64,2048]{1,0:T(8,128)(2,1)} reduce(bf16[4,64,2048]{2,1,0:T(8,128)(2,1)} %all-to-all-done.1, bf16[]{:T(256)} %constant.69.clone.1), dimensions={0}, to_apply=%region_3.4 | reduce | flops 393216 | bytes 1310722 | tf_op jit(solution)/shard_map/reduce_sum | solution.py:415
  (98 shorter events, 44.2 us)
Async XLA Ops:
  0.6 9.6 %collective-permute-start = (bf16[64,2048]{1,0:T(8,128)(2,1)}, bf16[64,2048]{1,0:T(8,128)(2,1)S(1)}, u32[]{:S(2)}, u32[]{:S(2)}) collective-permute-start(bf16[64,2048]{1,0:T(8,128)(2,1)} %own_ref.1), channel_id=1, source_target_pairs={{0,1},{1,2},{2,3},{3,0},{4,5},{5,6},{6,7},{7,4},{8,9},{9,10},{10,1... | collective-permute-start | bytes 786440 | tf_op jit(solution)/shard_map/ppermute | solution.py:305
  2.3 13.1 %collective-permute-start.1 = (bf16[64,2048]{1,0:T(8,128)(2,1)}, bf16[64,2048]{1,0:T(8,128)(2,1)S(1)}, u32[]{:S(2)}, u32[]{:S(2)}) collective-permute-start(bf16[64,2048]{1,0:T(8,128)(2,1)} %own_ref.1), channel_id=1, source_target_pairs={{0,3},{1,0},{2,1},{3,2},{4,7},{5,4},{6,5},{7,6},{8,11},{9,8},{10,9... | collective-permute-start | bytes 786440 | tf_op jit(solution)/shard_map/ppermute | solution.py:305
  4.0 13.1 %collective-permute-start.2 = (bf16[64,2048]{1,0:T(8,128)(2,1)}, bf16[64,2048]{1,0:T(8,128)(2,1)S(1)}, u32[]{:S(2)}, u32[]{:S(2)}) collective-permute-start(bf16[64,2048]{1,0:T(8,128)(2,1)} %own_ref.1), channel_id=1, source_target_pairs={{0,2},{1,3},{2,0},{3,1},{4,6},{5,7},{6,4},{7,5},{8,10},{9,11},{10,... | collective-permute-start | bytes 786440 | tf_op jit(solution)/shard_map/ppermute | solution.py:305
  24.1 10.2 %collective-permute-start.3 = (bf16[2,128,256]{2,1,0:T(8,128)(2,1)S(1)}, bf16[2,128,256]{2,1,0:T(8,128)(2,1)}, u32[]{:S(2)}, u32[]{:S(2)}) collective-permute-start(bf16[2,128,256]{2,1,0:T(8,128)(2,1)S(1)} %pad_maximum_fusion.6), channel_id=1, source_target_pairs={{224,0},{228,4},{232,8},{236,12},{240,16},{244,20},{248,24},{252,2... | collective-permute-start | bytes 393224 | tf_op jit(solution)/shard_map/ppermute | solution.py:335
  26.5 11.2 %collective-permute-start.5 = (bf16[512,128]{1,0:T(8,128)(2,1)S(1)}, bf16[512,128]{1,0:T(8,128)(2,1)S(1)}, u32[]{:S(2)}, u32[]{:S(2)}) collective-permute-start(bf16[512,128]{1,0:T(8,128)(2,1)S(1)} %get-tuple-element.48.own_ref), channel_id=1, source_target_pairs={{0,8},{4,12},{8,16},{12,20},{16,24},{20,28},{24,0},{28,4},{32,40},... | collective-permute-start | bytes 393224 | tf_op jit(solution)/shard_map/ppermute | solution.py:27
  28.0 9.7 %collective-permute-start.6 = (bf16[512,128]{1,0:T(8,128)(2,1)S(1)}, bf16[512,128]{1,0:T(8,128)(2,1)S(1)}, u32[]{:S(2)}, u32[]{:S(2)}) collective-permute-start(bf16[512,128]{1,0:T(8,128)(2,1)S(1)} %get-tuple-element.48.own_ref), channel_id=1, source_target_pairs={{0,24},{4,28},{8,0},{12,4},{16,8},{20,12},{24,16},{28,20},{32,56},... | collective-permute-start | bytes 393224 | tf_op jit(solution)/shard_map/ppermute | solution.py:27
  28.6 9.2 %collective-permute-start.7 = (bf16[512,128]{1,0:T(8,128)(2,1)S(1)}, bf16[512,128]{1,0:T(8,128)(2,1)S(1)}, u32[]{:S(2)}, u32[]{:S(2)}) collective-permute-start(bf16[512,128]{1,0:T(8,128)(2,1)S(1)} %get-tuple-element.48.own_ref), channel_id=1, source_target_pairs={{0,16},{4,20},{8,24},{12,28},{16,0},{20,4},{24,8},{28,12},{32,48},... | collective-permute-start | bytes 393224 | tf_op jit(solution)/shard_map/ppermute | solution.py:27
  30.7 24.3 %collective-permute-start.8 = (bf16[4,128,256]{2,1,0:T(8,128)(2,1)S(1)}, bf16[4,128,256]{2,1,0:T(8,128)(2,1)S(1)}, u32[]{:S(2)}, u32[]{:S(2)}) collective-permute-start(bf16[4,128,256]{2,1,0:T(8,128)(2,1)S(1)} %bitcast.61), channel_id=1, source_target_pairs={{0,4},{4,0},{8,12},{12,8},{16,20},{20,16},{24,28},{28,24},{32,36},... | collective-permute-start | bytes 786440 | tf_op jit(solution)/shard_map/ppermute | solution.py:27
  35.8 6.7 %collective-permute-start.4 = (bf16[30,512]{1,0:T(8,128)(2,1)S(1)}, bf16[30,512]{1,0:T(8,128)(2,1)S(1)}, u32[]{:S(2)}, u32[]{:S(2)}) collective-permute-start(bf16[30,512]{1,0:T(8,128)(2,1)S(1)} %slice.353), channel_id=1, source_target_pairs={{0,4},{4,8},{8,12},{12,16},{16,20},{20,24},{24,28},{28,32},{32,36}... | collective-permute-start | bytes 92168 | tf_op jit(solution)/shard_map/ppermute | solution.py:37
  38.6 27.0 %collective-permute-start.10 = (bf16[2048,128]{1,0:T(8,128)(2,1)}, bf16[2048,128]{1,0:T(8,128)(2,1)}, u32[]{:S(2)}, u32[]{:S(2)}) collective-permute-start(bf16[2048,128]{1,0:T(8,128)(2,1)} %pad_maximum_fusion.1), channel_id=1, source_target_pairs={{0,32},{4,36},{8,40},{12,44},{16,48},{20,52},{24,56},{28,60},{32,6... | collective-permute-start | bytes 1572872 | tf_op jit(solution)/shard_map/ppermute | solution.py:27
  40.3 25.3 %collective-permute-start.11 = (bf16[2048,128]{1,0:T(8,128)(2,1)}, bf16[2048,128]{1,0:T(8,128)(2,1)}, u32[]{:S(2)}, u32[]{:S(2)}) collective-permute-start(bf16[2048,128]{1,0:T(8,128)(2,1)} %pad_maximum_fusion.1), channel_id=1, source_target_pairs={{0,224},{4,228},{8,232},{12,236},{16,240},{20,244},{24,248},{28,25... | collective-permute-start | bytes 1572872 | tf_op jit(solution)/shard_map/ppermute | solution.py:27
  41.2 13.8 %collective-permute-start.9 = (bf16[2,128,256]{2,1,0:T(8,128)(2,1)}, bf16[2,128,256]{2,1,0:T(8,128)(2,1)}, u32[]{:S(2)}, u32[]{:S(2)}) collective-permute-start(bf16[2,128,256]{2,1,0:T(8,128)(2,1)} %collective-permute-done.3), channel_id=1, source_target_pairs={{0,4},{4,0},{8,12},{12,8},{16,20},{20,16},{24,28},{28,24},{32,36},... | collective-permute-start | bytes 393224 | tf_op jit(solution)/shard_map/ppermute | solution.py:27
  46.5 8.5 %all-to-all-start = ((f32[4,1,512]{2,1,0:T(1,128)}), f32[4,1,512]{2,1,0:T(1,128)S(1)}, u32[]{:S(2)}, u32[]{:S(2)}) async-start(f32[4,1,512]{2,1,0:T(1,128)} %broadcast_in_dim.7), calls=%async_computation | async-start | bytes 16384 | tf_op jit(solution)/shard_map/all_to_all | solution.py:42
  65.6 15.9 %collective-permute-start.12 = (bf16[2048,128]{1,0:T(8,128)(2,1)}, bf16[2048,128]{1,0:T(8,128)(2,1)S(1)}, u32[]{:S(2)}, u32[]{:S(2)}) collective-permute-start(bf16[2048,128]{1,0:T(8,128)(2,1)} %collective-permute-done.10.a_ref), channel_id=1, source_target_pairs={{0,32},{4,36},{8,40},{12,44},{16,48},{20,52},{24,56},{28,60},{32,6... | collective-permute-start | bytes 1572872 | tf_op jit(solution)/shard_map/ppermute | solution.py:27
  66.5 15.0 %collective-permute-start.13 = (bf16[2048,128]{1,0:T(8,128)(2,1)}, bf16[2048,128]{1,0:T(8,128)(2,1)S(1)}, u32[]{:S(2)}, u32[]{:S(2)}) collective-permute-start(bf16[2048,128]{1,0:T(8,128)(2,1)} %collective-permute-done.11.b_ref), channel_id=1, source_target_pairs={{0,224},{4,228},{8,232},{12,236},{16,240},{20,244},{24,248},{28,25... | collective-permute-start | bytes 1572872 | tf_op jit(solution)/shard_map/ppermute | solution.py:27
  81.5 13.0 %collective-permute-start.14 = (bf16[2048,128]{1,0:T(8,128)(2,1)S(1)}, bf16[2048,128]{1,0:T(8,128)(2,1)S(1)}, u32[]{:S(2)}, u32[]{:S(2)}) collective-permute-start(bf16[2048,128]{1,0:T(8,128)(2,1)S(1)} %collective-permute-done.12.a_ref), channel_id=1, source_target_pairs={{0,32},{4,36},{8,40},{12,44},{16,48},{20,52},{24,56},{28,60},{32,6... | collective-permute-start | bytes 1572872 | tf_op jit(solution)/shard_map/ppermute | solution.py:27
  81.6 12.9 %collective-permute-start.15 = (bf16[2048,128]{1,0:T(8,128)(2,1)S(1)}, bf16[2048,128]{1,0:T(8,128)(2,1)S(1)}, u32[]{:S(2)}, u32[]{:S(2)}) collective-permute-start(bf16[2048,128]{1,0:T(8,128)(2,1)S(1)} %collective-permute-done.13.b_ref), channel_id=1, source_target_pairs={{0,224},{4,228},{8,232},{12,236},{16,240},{20,244},{24,248},{28,25... | collective-permute-start | bytes 1572872 | tf_op jit(solution)/shard_map/ppermute | solution.py:27
  94.5 8.3 %collective-permute-start.16 = (bf16[1024,128]{1,0:T(8,128)(2,1)S(1)}, bf16[1024,128]{1,0:T(8,128)(2,1)S(1)}, u32[]{:S(2)}, u32[]{:S(2)}) collective-permute-start(bf16[1024,128]{1,0:T(8,128)(2,1)S(1)} %slice.335), channel_id=1, source_target_pairs={{0,32},{4,36},{8,40},{12,44},{16,48},{20,52},{24,56},{28,60},{32,6... | collective-permute-start | bytes 786440 | tf_op jit(solution)/shard_map/ppermute | solution.py:27
  96.8 6.4 %collective-permute-start.17 = (bf16[1024,128]{1,0:T(8,128)(2,1)S(1)}, bf16[1024,128]{1,0:T(8,128)(2,1)S(1)}, u32[]{:S(2)}, u32[]{:S(2)}) collective-permute-start(bf16[1024,128]{1,0:T(8,128)(2,1)S(1)} %slice.336), channel_id=1, source_target_pairs={{0,224},{4,228},{8,232},{12,236},{16,240},{20,244},{24,248},{28,25... | collective-permute-start | bytes 786440 | tf_op jit(solution)/shard_map/ppermute | solution.py:27
  108.6 3.8 %collective-permute-start.19 = (f32[12,128,256]{2,1,0:T(8,128)}, f32[12,128,256]{2,1,0:T(8,128)}, u32[]{:S(2)}, u32[]{:S(2)}) collective-permute-start(f32[12,128,256]{2,1,0:T(8,128)} %get-tuple-element.87), channel_id=1, source_target_pairs={{0,4},{4,0},{8,12},{12,8},{16,20},{20,16},{24,28},{28,24},{32,36},... | collective-permute-start | bytes 4718600 | tf_op jit(solution)/shard_map/ppermute | solution.py:27
  109.3 3.1 %collective-permute-start.18 = (f32[12,8,256]{2,1,0:T(8,128)S(1)}, f32[12,8,256]{2,1,0:T(8,128)S(1)}, u32[]{:S(2)}, u32[]{:S(2)}) collective-permute-start(f32[12,8,256]{2,1,0:T(8,128)S(1)} %get-tuple-element.86), channel_id=1, source_target_pairs={{0,4},{4,0},{8,12},{12,8},{16,20},{20,16},{24,28},{28,24},{32,36},... | collective-permute-start | bytes 294920 | tf_op jit(solution)/shard_map/ppermute | solution.py:27
  115.7 18.9 %collective-permute-start.20 = (bf16[2,128,256]{2,1,0:T(8,128)(2,1)S(1)}, bf16[2,128,256]{2,1,0:T(8,128)(2,1)S(1)}, u32[]{:S(2)}, u32[]{:S(2)}) collective-permute-start(bf16[2,128,256]{2,1,0:T(8,128)(2,1)S(1)} %get-tuple-element.98), channel_id=1, source_target_pairs={{0,224},{4,228},{8,232},{12,236},{16,240},{20,244},{24,248},{28,25... | collective-permute-start | bytes 393224 | tf_op jit(solution)/shard_map/ppermute | solution.py:398
  138.6 19.1 %all-to-all-start.1 = ((bf16[4,64,2048]{2,1,0:T(8,128)(2,1)}), bf16[4,64,2048]{2,1,0:T(8,128)(2,1)}, u32[]{:S(2)}, u32[]{:S(2)}) async-start(bf16[4,64,2048]{2,1,0:T(8,128)(2,1)} %bitcast.45), calls=%async_computation.1 | async-start | bytes 2097152 | tf_op jit(solution)/shard_map/all_to_all | solution.py:414
  142.9 8.7 %collective-permute-start.21 = (f32[2,2,256]{2,0,1:T(2,128)S(1)}, f32[2,2,256]{2,0,1:T(2,128)S(1)}, u32[]{:S(2)}, u32[]{:S(2)}) collective-permute-start(f32[2,2,256]{2,0,1:T(2,128)S(1)} %copy.42), channel_id=1, source_target_pairs={{0,224},{4,228},{8,232},{12,236},{16,240},{20,244},{24,248},{28,25... | collective-permute-start | bytes 12296 | tf_op jit(solution)/shard_map/ppermute | solution.py:399
  (15 other events, 161.4 us)

commit v3 on v2

--- a/solution.py
+++ b/solution.py
@@ -48,7 +48,7 @@
     return [(ref, row) for ref in pieces for row in range(0, ref.shape[0], 512)]
 
 
-def slab_pass(chunks, q_ref, state, s_refs, bias_ref, lo, hi):
+def slab_pass(chunks, q_ref, state, s_refs, bias_ref, lo, hi, plane=None):
     def score(pair, which, at):
         ref, row = chunks[at]
         keys = ref[row : row + 256, :]
@@ -58,7 +58,7 @@
             preferred_element_type=jnp.float32,
         )
         if bias_ref is not None:
-            s = s + bias_ref[which, at * 256 : at * 256 + 256, :]
+            s = s + bias_ref[plane(pair, which), at * 256 : at * 256 + 256, :]
         s_refs[which][at * 256 : at * 256 + 256, :] = s
         return jnp.max(s.reshape(32, 8, 256), axis=0)
 
@@ -91,11 +91,13 @@
         top = part if top is None else jnp.maximum(top, part)
 
     def some(i, top):
-        pair = lo + i
-        top = both(pair, 0, top, pair)
-        return both(pair, 1, top, jnp.minimum(pair + 1, hi - 1))
-
-    lax.fori_loop(0, hi - lo, some, top)
+        for j in range(2):
+            pair = lo + 2 * i + j
+            top = both(pair, 0, top, pair)
+            top = both(pair, 1, top, jnp.minimum(pair + 1, hi - 1))
+        return top
+
+    lax.fori_loop(0, (hi - lo) // 2, some, top)
 
 
 def spread_queries(q_in, q_ref):
@@ -120,6 +122,7 @@
 
 def fill_bias(where_ref, bias_ref):
     x, core = where_ref[1], where_ref[2]
+    bias_ref[2] = jnp.zeros((1024, 256), jnp.float32)
     key_at = lax.broadcasted_iota(jnp.int32, (256, 256), 0)
     query_at = lax.broadcasted_iota(jnp.int32, (256, 256), 1)
     bias_ref[0, 0:256, :] = jnp.where(key_at <= query_at, 0.0, NEG)
@@ -131,7 +134,7 @@
 
 
 def first_kernel(where_ref, q_in, own_ref, left_ref, right_ref, far_ref, *rest):
-    state, (q_ref, s_a, s_b, bias_ref) = rest[:4], rest[4:]
+    state, (q_ref, s_a, s_b, bias_ref) = rest[:4], rest[4:8]
     spread_queries(q_in, q_ref)
     for stats_ref, o_ref in zip(state[:2], state[2:]):
         stats_ref[...] = jnp.zeros_like(stats_ref)
@@ -141,37 +144,34 @@
     fill_bias(where_ref, bias_ref)
     own_end, guest_end = work_ends(where_ref[0])
     chunks = chunk_refs((own_ref, left_ref, right_ref, far_ref))
-    slab_pass(chunks, q_ref, state, (s_a, s_b), bias_ref, 0, own_end)
-
-    @pl.when(guest_end > 8)
-    def _():
-        slab_pass(chunks, q_ref, state, (s_a, s_b), None, 8, guest_end)
-
-
-def slab_kernel(step, where_ref, q_in, a_ref, b_ref, *rest):
-    state, (q_ref, s_a, s_b, bias_ref) = rest[4:8], rest[8:]
+    plane = lambda pair, which: jnp.where(pair < 8, which, 2)
+    end = jnp.where(guest_end > 8, guest_end, own_end)
+    slab_pass(chunks, q_ref, state, (s_a, s_b), bias_ref, 0, end, plane)
+
+
+def slab_kernel(step, where_ref, q_ref, a_ref, b_ref, *rest):
+    state, (s_a, s_b, bias_ref) = rest[4:8], rest[8:]
     for before, after in zip(rest[:4], state):
         after[...] = before[...]
     z = where_ref[0]
-    spread_queries(q_in, q_ref)
     own_end, guest_end = work_ends(z)
+    if step in (1, 3):
+        fill_bias(where_ref, bias_ref)
 
     def go(slab, masked, *pieces):
         chunks = chunk_refs(pieces)
         own_seen, guest_seen = slab < z, (slab < 7 - z) & (z < 4)
         lo = jnp.where(own_seen, 0, 8)
         hi = jnp.where(guest_seen, guest_end, jnp.where(own_seen, own_end, 8))
+        same = (slab == 7 - z) & (guest_end > 8)
+        if masked:
+            hi = jnp.where(same, guest_end, hi)
 
         @pl.when(hi > lo)
         def _():
-            slab_pass(chunks, q_ref, state, (s_a, s_b), None, lo, hi)
-
-        if masked:
-
-            @pl.when((slab == 7 - z) & (guest_end > 8))
-            def _():
-                fill_bias(where_ref, bias_ref)
-                slab_pass(chunks, q_ref, state, (s_a, s_b), bias_ref, 8, guest_end)
+            plane = lambda pair, which: jnp.where(same, which, 2)
+            bias = bias_ref if masked else None
+            slab_pass(chunks, q_ref, state, (s_a, s_b), bias, lo, hi, plane)
 
     below, above = lax.rem(z + 8 - step, 8), lax.rem(z + step, 8)
     if step == 4:
@@ -182,31 +182,34 @@
 
 
 VMEM_SPEC = pl.BlockSpec(memory_space=pltpu.VMEM)
+HBM_SPEC = pl.BlockSpec(memory_space=pltpu.HBM)
 SMEM_SPEC = pl.BlockSpec(memory_space=pltpu.SMEM)
 
 
-def plain_kernel(body, name, args, out_shape, scratch=(), aliases={}, flops=1 << 28, smem=1):
+def plain_kernel(
+    body, name, args, out_shape, scratch=(), aliases={}, flops=1 << 28, smem=1, spec=pl.BlockSpec(),
+    vmem=24, hbm=0
+):
     return pl.pallas_call(
         body,
         out_shape=out_shape,
-        in_specs=[SMEM_SPEC] * smem + [VMEM_SPEC] * (len(args) - smem),
-        out_specs=jax.tree.map(lambda _: VMEM_SPEC, out_shape),
+        in_specs=[SMEM_SPEC] * smem + [HBM_SPEC] * hbm + [spec] * (len(args) - smem - hbm),
+        out_specs=jax.tree.map(lambda _: spec, out_shape),
         scratch_shapes=scratch,
         input_output_aliases=aliases,
-        compiler_params=pltpu.CompilerParams(vmem_limit_bytes=24 << 20),
+        compiler_params=pltpu.CompilerParams(vmem_limit_bytes=vmem << 20),
         cost_estimate=pl.CostEstimate(flops=flops, bytes_accessed=2 << 20, transcendentals=0),
         name=name,
     )(*args)
 
 
 def attend(where, q, pieces, state, step):
-    units = q.shape[0]
+    units = 24
     shapes = [(units // 2, 8, 256)] * 2 + [(units // 2, 128, 256)] * 2
     scratch = [
-        pltpu.VMEM((units, 256, 256), jnp.bfloat16),
         pltpu.VMEM((1024, 256), jnp.float32),
         pltpu.VMEM((1024, 256), jnp.float32),
-        pltpu.VMEM((2, 1024, 256), jnp.float32),
+        pltpu.VMEM((3, 1024, 256), jnp.float32),
     ]
     if step == 0:
         body, args, aliases, keys = first_kernel, (where, q, *pieces), {}, 1024
@@ -216,19 +219,33 @@
         keys = sum(p.shape[0] for p in pieces) // 2
     kind = jax.ShapeDtypeStruct if step == 4 else pltpu.VMEM
     out_shape = tuple(kind(s, jnp.float32) for s in shapes)
+    if step == 0:
+        out_shape = (*out_shape, pltpu.VMEM((units, 256, 256), jnp.bfloat16))
     flops = keys * 256 * units * 256
-    return plain_kernel(body, f"attend_{step}", args, out_shape, scratch, aliases, flops)
-
-
-def front_kernel(where_ref, own_ref, left_ref, right_ref, far_ref, gain_ref, wk_ref, wv_ref, key_gain_ref, normed_ref, kv_ref):
+    return plain_kernel(
+        body, f"attend_{step}", args, out_shape, scratch, aliases, flops, spec=VMEM_SPEC
+    )
+
+
+def front_kernel(where_ref, *refs):
+    (left_ref, right_ref, far_ref, normed_ref, kv_ref), held = refs[5:10], refs[10:15]
+    own_ref, gain_ref, wk_ref, wv_ref, key_gain_ref = held
+    copies = [pltpu.make_async_copy(refs[k], held[k], refs[15].at[k]) for k in range(5)]
+    for k in (1, 0, 2, 3, 4):
+        copies[k].start()
     t = where_ref[3]
-    for ref, step in ((own_ref, 0), (left_ref, 3), (right_ref, 1), (far_ref, 2)):
+    copies[1].wait()
+    for ref, step in ((left_ref, 3), (right_ref, 1), (far_ref, 2), (own_ref, 0)):
+        if step == 0:
+            copies[0].wait()
         row = pl.multiple_of(lax.rem(t + step, 4) * 64, 64)
         rows = ref[...].astype(jnp.float32)
         mean = jnp.mean(rows * rows, axis=1, keepdims=True)
         normed_ref[pl.ds(row, 64), :] = (rows * lax.rsqrt(mean + 1e-06) * gain_ref[...]).astype(
             jnp.bfloat16
         )
+    for k in (2, 3, 4):
+        copies[k].wait()
     normed = normed_ref[...]
     keys = jnp.dot(normed, wk_ref[...], preferred_element_type=jnp.float32)
     first = lax.broadcasted_iota(jnp.int32, keys.shape, 1) < 64
@@ -271,7 +288,7 @@
             l_all = stats_a[pair, 1:2, :] * w_a + stats_b[pair, 1:2, :] * w_b
             log_ref[pair, 0:1, :] = m_all * LN2 + jnp.log(l_all)
             maps.append((acc_a[pair] * w_a + acc_b[pair] * w_b) * (1.0 / l_all))
-        diff = maps[0] - lam_ref[head] * maps[1]
+        diff = maps[0] - lam_ref[(0, 1, 2, 3, 3, 2)[head]] * maps[1]
         mean = jnp.mean(diff * diff, axis=0, keepdims=True)
         head_ref[head] = (diff * lax.rsqrt(mean + 1e-06) * gain_ref[...]).astype(jnp.bfloat16)
 
@@ -311,15 +328,24 @@
         (
             where,
             tokens,
-            rows_of[1],
-            rows_of[2],
-            rows_of[0],
             norm_gain[None],
             w_key,
             w_value,
             key_gain,
+            rows_of[1],
+            rows_of[2],
+            rows_of[0],
         ),
         (normed_shape, jax.ShapeDtypeStruct((512, 128), jnp.bfloat16)),
+        scratch=[
+            pltpu.VMEM(tokens.shape, jnp.bfloat16),
+            pltpu.VMEM((1, tokens.shape[1]), jnp.float32),
+            pltpu.VMEM(w_key.shape, jnp.bfloat16),
+            pltpu.VMEM(w_value.shape, jnp.bfloat16),
+            pltpu.VMEM(key_gain.shape, jnp.float32),
+            pltpu.SemaphoreType.DMA((5,)),
+        ],
+        hbm=5,
     )
 
     query_t = plain_kernel(
@@ -371,24 +397,30 @@
 
     where_2, out_part = lax.optimization_barrier((where, out_part))
 
-    state = attend(where_0, both_q, (own, left, right, far), None, 0)
+    *state, spread_q = attend(where, both_q, (own, left, right, far), None, 0)
     for step in range(1, 5):
-        up, down, first = lax.optimization_barrier((up, down, state[0]))
-        state = (first, *state[1:])
+        held = sums if step == 1 else behind
+        up, down, held = lax.optimization_barrier((up, down, held))
+        if step > 1:
+            state = (held, *state[1:])
         if step < 4:
             new_up = sp_send(up if step < 3 else up[:1024], lambda z, x, c: (z + 1, x, c))
             new_down = sp_send(down if step < 3 else down[1024:], lambda z, x, c: (z - 1, x, c))
-        state = attend(where if step == 1 else where_2, both_q, (up, down), state, step)
+        behind = state[0]
+        if step > 1:
+            state = attend(where_2 if step == 3 else where, spread_q, pending, state, step - 1)
+            behind = state[0]
+        pending = (up, down)
         if step < 4:
             up, down = new_up, new_down
+    state = attend(where_2, spread_q, pending, state, 4)
 
     other_stats, other_acc = sp_send(state[1], swap), sp_send(state[3], swap)
-    lam_all = jnp.concatenate([lam_head, lam_head[3:], lam_head[2:3]])
     pairs = state[0].shape[0]
     head_out, logs = plain_kernel(
         finish_kernel,
         "finish",
-        (lam_all, sub_gain[:, None], state[0], state[2], other_stats, other_acc),
+        (lam_head, sub_gain[:, None], state[0], state[2], other_stats, other_acc),
         (
             jax.ShapeDtypeStruct((pairs // 2, 128, tok_dev), jnp.bfloat16),
             jax.ShapeDtypeStruct((pairs, 8, tok_dev), jnp.float32),

time: 161 us -> 155 us (0.963)
  Pallas kernels: 37.4 us -> 33.6 us
  starting transfers between devices: 58.9 us -> 55.6 us
  waiting for transfers between devices: 33.1 us -> 35.9 us
    pallas_call x8, Pallas kernels: 37.4 us -> 33.6 us  [plain_kernel(): pl.pallas_call(body, out_shape=out_shape, in_specs=[SMEM_SPEC] * smem + [...]
    ppermute x15, starting transfers between devices: 19.4 us -> 16.8 us  [sp_send(): return lax.ppermute(value, 'sp', sp_table(move))]
    ppermute x15, waiting for transfers between devices: 6.54 us -> 9.1 us  [sp_send(): return lax.ppermute(value, 'sp', sp_table(move))]
  transfers between devices with their start and end apart: 24 -> 24, of which waited for: 11 -> 14; matrix products, arithmetic and copies ran while one was open for 10% -> 9% of each run, Pallas kernels for 18% -> 14%
where the time goes in v3:
time: 155 us; the launch traced here: 154 us
  starting transfers between devices  55.6 us (36%)
  waiting for transfers between devices  35.9 us (23%)
  Pallas kernels  33.6 us (22%)
  local copies, waits for them, and re-layouts  10.9 us (7%)
  other arithmetic  9.09 us (6%)
  matrix products  7.64 us (5%)
    pallas_call x8, Pallas kernels, plain_kernel(): pl.pallas_call(body, out_shape=out_shape, in_specs=[SMEM_SPEC] * smem + [...  33.6 us
    ppermute x15, starting transfers between devices, sp_send(): return lax.ppermute(value, 'sp', sp_table(move))  16.8 us
    ppermute x1, starting transfers between devices, on_device(): back_out = lax.ppermute(head_out[heads:], 'sp', mirrored((0, 1, 2)))  15.4 us
    ppermute x15, waiting for transfers between devices, sp_send(): return lax.ppermute(value, 'sp', sp_table(move))  9.1 us
    ppermute x3, waiting for transfers between devices, on_device(): lax.ppermute(tokens, 'tp', [(t, (t + step) % 4) for t in range(4)])  9.1 us
    ppermute x1, starting transfers between devices, on_device(): back_logs = lax.ppermute(logs[heads:], 'sp', mirrored((0, 1, 2)))  7.39 us
    unnamed x30, local copies, waits for them, and re-layouts  7.01 us
    all_to_all x1, waiting for transfers between devices, on_device(): lax.all_to_all(out_part.reshape(tp_count, -1, out_part.shape[1]), 'tp', 0...  5.49 us
  transfers between devices with their start and end apart: 24, of which 14 were waited for; matrix products, arithmetic and copies ran while one was open for 9% of the time, Pallas kernels for 14%

profile of v3, /device:TPU:34, one launch (start us, length us, event | category | flops | bytes accessed | tf_op | source)
XLA Modules:
  0.0 153.7 jit_solution(11341350963012013078)
XLA Ops:
  4.0 2.0 %collective-permute-start.2 = (bf16[64,2048]{1,0:T(8,128)(2,1)}, bf16[64,2048]{1,0:T(8,128)(2,1)S(1)}, u32[]{:S(2)}, u32[]{:S(2)}) collective-permute-start(bf16[64,2048]{1,0:T(8,128)(2,1)} %refs_0_.1), channel_id=1, source_target_pairs={{0,2},{1,3},{2,0},{3,1},{4,6},{5,7},{6,4},{7,5},{8,10},{9,11},{10,... | collective-permute-start | bytes 786440 | tf_op jit(solution)/shard_map/ppermute | solution.py:322
  7.9 2.3 %collective-permute-done.refs_5_ = bf16[64,2048]{1,0:T(8,128)(2,1)S(1)} collective-permute-done((bf16[64,2048]{1,0:T(8,128)(2,1)}, bf16[64,2048]{1,0:T(8,128)(2,1)S(1)}, u32[]{:S(2)}, u32[]{:S(2)}) %collective-permute-start) | collective-permute-done | bytes 262176 | tf_op jit(solution)/shard_map/ppermute | solution.py:322
  10.3 5.1 %collective-permute-done.1.refs_6_ = bf16[64,2048]{1,0:T(8,128)(2,1)S(1)} collective-permute-done((bf16[64,2048]{1,0:T(8,128)(2,1)}, bf16[64,2048]{1,0:T(8,128)(2,1)S(1)}, u32[]{:S(2)}, u32[]{:S(2)}) %collective-permute-start.1) | collective-permute-done | bytes 262176 | tf_op jit(solution)/shard_map/ppermute | solution.py:322
  28.8 2.1 %collective-permute-start.7 = (bf16[512,128]{1,0:T(8,128)(2,1)S(1)}, bf16[512,128]{1,0:T(8,128)(2,1)S(1)}, u32[]{:S(2)}, u32[]{:S(2)}) collective-permute-start(bf16[512,128]{1,0:T(8,128)(2,1)S(1)} %get-tuple-element.47.own_ref), channel_id=1, source_target_pairs={{0,16},{4,20},{8,24},{12,28},{16,0},{20,4},{24,8},{28,12},{32,48},... | collective-permute-start | bytes 393224 | tf_op jit(solution)/shard_map/ppermute | solution.py:27
  31.0 3.5 %collective-permute-done.3 = bf16[2,128,256]{2,1,0:T(8,128)(2,1)} collective-permute-done((bf16[2,128,256]{2,1,0:T(8,128)(2,1)S(1)}, bf16[2,128,256]{2,1,0:T(8,128)(2,1)}, u32[]{:S(2)}, u32[]{:S(2)}) %collective-permute-start.3) | collective-permute-done | bytes 131104 | tf_op jit(solution)/shard_map/ppermute | solution.py:361
  42.8 3.3 %fusion.40 = (f32[256]{0:T(256)S(1)}, f32[256]{0:T(256)S(1)}, f32[256,512]{1,0:T(8,128)}) fusion(bf16[256,512]{1,0:T(8,128)(2,1)S(1)} %fusion.4, f32[512]{0:T(512)S(1)} %bitcast.97, bf16[30,512]{1,0:T(8,128)(2,1)S(1)} %collective-permute-done.4, f32[512]{0:T(512)S(1)} %bitcast.98, f32[512]{0:T(512)S(1)} %bitcast.69, f32[512]{0:T(512)S(1)} %bitcast.70, ...), kind=kLoop, calls=%fused_computation.103 | loop fusion | flops 24247808 | bytes 882688 | tf_op jit(solution)/shard_map/reduce_sum | solution.py:388
  46.7 3.2 %all-to-all-start = ((f32[4,1,512]{2,1,0:T(1,128)}), f32[4,1,512]{2,1,0:T(1,128)S(1)}, u32[]{:S(2)}, u32[]{:S(2)}) async-start(f32[4,1,512]{2,1,0:T(1,128)} %broadcast_in_dim.7), calls=%async_computation | async-start | bytes 16384 | tf_op jit(solution)/shard_map/all_to_all | solution.py:42
  50.9 4.3 %all-to-all-done = f32[4,1,512]{2,1,0:T(1,128)S(1)} async-done(((f32[4,1,512]{2,1,0:T(1,128)}), f32[4,1,512]{2,1,0:T(1,128)S(1)}, u32[]{:S(2)}, u32[]{:S(2)}) %all-to-all-start) | async-done | bytes 8224 | tf_op jit(solution)/shard_map/all_to_all | solution.py:42
  56.4 2.2 %collective-permute-start.13 = (bf16[2048,128]{1,0:T(8,128)(2,1)}, bf16[2048,128]{1,0:T(8,128)(2,1)S(1)}, u32[]{:S(2)}, u32[]{:S(2)}) collective-permute-start(bf16[2048,128]{1,0:T(8,128)(2,1)} %collective-permute-done.11.b_ref), channel_id=1, source_target_pairs={{0,224},{4,228},{8,232},{12,236},{16,240},{20,244},{24,248},{28,25... | collective-permute-start | bytes 1572872 | tf_op jit(solution)/shard_map/ppermute | solution.py:27
  59.7 8.9 %attend_0.1 = (f32[12,8,256]{2,1,0:T(8,128)S(1)}, f32[12,8,256]{2,1,0:T(8,128)S(1)}, f32[12,128,256]{2,1,0:T(8,128)S(1)}, f32[12,128,256]{2,1,0:T(8,128)S(1)}, bf16[24,256,256]{2,1,0:T(8,128)(2,1)S(1)}) custom-call(s32[4]{0:T(128)S(1)} %pad_add_fusion.where_ref, bf16[24,64,256]{2,1,0:T(8,128)(2,1)S(1)} %bitcast.63, ...), custom_call_target="tpu_custom_call" | custom-call | flops 1610612736 | bytes 2097152 | tf_op jit(solution)/shard_map/attend_0/pallas_call | solution.py:193
  73.4 2.2 %fusion.5 = f32[256,2048]{1,0:T(8,128)} fusion(bf16[512,2048]{1,0:T(8,128)(2,1)S(1)} %copy-done, f32[256,512]{1,0:T(8,128)S(1)} %copy-done.11, f32[512]{0:T(512)S(1)} %copy-done.14, f32[256]{0:T(256)S(1)} %get-tuple-element.133, f32[256]{0:T(256)S(1)} %get-tuple-element.132), kind=kOutput, calls=%fused_computation.44 | convolution fusion | flops 537919488 | bytes 4722688 | tf_op jit(solution)/shard_map/dot_general | solution.py:396
  75.6 9.6 %attend_1.1 = (f32[12,8,256]{2,1,0:T(8,128)S(1)}, f32[12,8,256]{2,1,0:T(8,128)S(1)}, f32[12,128,256]{2,1,0:T(8,128)S(1)}, f32[12,128,256]{2,1,0:T(8,128)S(1)}) custom-call(s32[4]{0:T(128)S(1)} %pad_add_fusion.where_ref, bf16[24,256,256]{2,1,0:T(8,128)(2,1)S(1)} %get-tuple-element.53.q_ref, ...), custom_call_target="tpu_custom_call", output_to_operand_aliasing={{0}: (4, {}), {1}: (5, {}), {2}: (6, {}), {3}: (7, {})} | custom-call | flops 3221225472 | bytes 2097152 | tf_op jit(solution)/shard_map/attend_1/pallas_call | solution.py:193
  87.8 2.7 %attend_2.1 = (f32[12,8,256]{2,1,0:T(8,128)S(1)}, f32[12,8,256]{2,1,0:T(8,128)S(1)}, f32[12,128,256]{2,1,0:T(8,128)S(1)}, f32[12,128,256]{2,1,0:T(8,128)S(1)}) custom-call(s32[4]{0:T(128)S(1)} %pad_add_fusion.where_ref, bf16[24,256,256]{2,1,0:T(8,128)(2,1)S(1)} %get-tuple-element.53.q_ref, ...), custom_call_target="tpu_custom_call", output_to_operand_aliasing={{0}: (4, {}), {1}: (5, {}), {2}: (6, {}), {3}: (7, {})} | custom-call | flops 3221225472 | bytes 2097152 | tf_op jit(solution)/shard_map/attend_2/pallas_call | solution.py:193
  93.9 4.1 %attend_3.1 = (f32[12,8,256]{2,1,0:T(8,128)S(1)}, f32[12,8,256]{2,1,0:T(8,128)S(1)}, f32[12,128,256]{2,1,0:T(8,128)S(1)}, f32[12,128,256]{2,1,0:T(8,128)S(1)}) custom-call(s32[4]{0:T(128)S(1)} %pad_add_fusion.where_ref, bf16[24,256,256]{2,1,0:T(8,128)(2,1)S(1)} %get-tuple-element.53.q_ref, ...), custom_call_target="tpu_custom_call", output_to_operand_aliasing={{0}: (4, {}), {1}: (5, {}), {2}: (6, {}), {3}: (7, {})} | custom-call | flops 3221225472 | bytes 2097152 | tf_op jit(solution)/shard_map/attend_3/pallas_call | solution.py:193
  98.0 3.6 %attend_4.1 = (f32[12,8,256]{2,1,0:T(8,128)S(1)}, f32[12,8,256]{2,1,0:T(8,128)S(1)}, f32[12,128,256]{2,1,0:T(8,128)S(1)}, f32[12,128,256]{2,1,0:T(8,128)}) custom-call(s32[4]{0:T(128)S(1)} %pad_add_fusion.where_ref, bf16[24,256,256]{2,1,0:T(8,128)(2,1)S(1)} %get-tuple-element.53.q_ref, bf16[1024,128]{1,0:T(8,128)(2,1)S(1)} %collective-permute-done.16.a_ref, ...), custom_call_target="tpu_custom_call" | custom-call | flops 1610612736 | bytes 2097152 | tf_op jit(solution)/shard_map/attend_4/pallas_call | solution.py:193
  103.4 3.1 %collective-permute-done.18.stats_b = f32[12,8,256]{2,1,0:T(8,128)S(1)} collective-permute-done((f32[12,8,256]{2,1,0:T(8,128)S(1)}, f32[12,8,256]{2,1,0:T(8,128)S(1)}, u32[]{:S(2)}, u32[]{:S(2)}) %collective-permute-start.18) | collective-permute-done | bytes 98336 | tf_op jit(solution)/shard_map/ppermute | solution.py:27
  107.9 1.9 %finish.1 = (bf16[6,128,256]{2,1,0:T(8,128)(2,1)S(1)}, f32[12,8,256]{2,1,0:T(8,128)S(1)}) custom-call(f32[4]{0:T(128)S(1)} %copy-done.8, f32[128,1]{1,0:T(8,128)S(1)} %copy.41.gain_ref, f32[12,8,256]{2,1,0:T(8,128)S(1)} %get-tuple-element.82.stats_a, f32[12,128,256]{2,1,0:T(8,128)S(1)} %copy-done.3, f32[12,8,256]{2,1,0:T(8,128)S(1)} %collective-permute-done.18.stats_b, ...), custom_call_target="tpu_custom_call" | custom-call | flops 268435456 | bytes 2097152 | tf_op jit(solution)/shard_map/finish/pallas_call | solution.py:193
  109.9 15.4 %collective-permute-start.20 = (bf16[2,128,256]{2,1,0:T(8,128)(2,1)S(1)}, bf16[2,128,256]{2,1,0:T(8,128)(2,1)S(1)}, u32[]{:S(2)}, u32[]{:S(2)}) collective-permute-start(bf16[2,128,256]{2,1,0:T(8,128)(2,1)S(1)} %get-tuple-element.96), channel_id=1, source_target_pairs={{0,224},{4,228},{8,232},{12,236},{16,240},{20,244},{24,248},{28,25... | collective-permute-start | bytes 393224 | tf_op jit(solution)/shard_map/ppermute | solution.py:430
  125.4 3.0 %collective-permute-done.20 = bf16[2,128,256]{2,1,0:T(8,128)(2,1)S(1)} collective-permute-done((bf16[2,128,256]{2,1,0:T(8,128)(2,1)S(1)}, bf16[2,128,256]{2,1,0:T(8,128)(2,1)S(1)}, u32[]{:S(2)}, u32[]{:S(2)}) %collective-permute-start.20) | collective-permute-done | bytes 131104 | tf_op jit(solution)/shard_map/ppermute | solution.py:430
  128.5 3.9 %fusion = bf16[256,2048]{1,0:T(8,128)(2,1)} fusion(f32[256,2048]{1,0:T(8,128)} %fusion.5, bf16[512,256]{1,0:T(8,128)(2,1)S(1)} %bitcast.67, bf16[512,2048]{1,0:T(8,128)(2,1)} %param.29), kind=kOutput, calls=%fused_computation.30 | convolution fusion | flops 537919488 | bytes 5505024 | tf_op jit(solution)/shard_map/dot_general | solution.py:442
  132.4 4.2 %all-to-all-start.1 = ((bf16[4,64,2048]{2,1,0:T(8,128)(2,1)}), bf16[4,64,2048]{2,1,0:T(8,128)(2,1)}, u32[]{:S(2)}, u32[]{:S(2)}) async-start(bf16[4,64,2048]{2,1,0:T(8,128)(2,1)} %bitcast.45), calls=%async_computation.1 | async-start | bytes 2097152 | tf_op jit(solution)/shard_map/all_to_all | solution.py:446
  136.7 7.4 %collective-permute-start.21 = (f32[2,2,256]{2,0,1:T(2,128)S(1)}, f32[2,2,256]{2,0,1:T(2,128)S(1)}, u32[]{:S(2)}, u32[]{:S(2)}) collective-permute-start(f32[2,2,256]{2,0,1:T(2,128)S(1)} %copy.42), channel_id=1, source_target_pairs={{0,224},{4,228},{8,232},{12,236},{16,240},{20,244},{24,248},{28,25... | collective-permute-start | bytes 12296 | tf_op jit(solution)/shard_map/ppermute | solution.py:431
  146.0 5.5 %all-to-all-done.1 = bf16[4,64,2048]{2,1,0:T(8,128)(2,1)} async-done(((bf16[4,64,2048]{2,1,0:T(8,128)(2,1)}), bf16[4,64,2048]{2,1,0:T(8,128)(2,1)}, u32[]{:S(2)}, u32[]{:S(2)}) %all-to-all-start.1) | async-done | bytes 1048608 | tf_op jit(solution)/shard_map/all_to_all | solution.py:446
  151.5 2.2 %reduce_sum.42 = bf16[64,2048]{1,0:T(8,128)(2,1)} reduce(bf16[4,64,2048]{2,1,0:T(8,128)(2,1)} %all-to-all-done.1, bf16[]{:T(256)} %constant.69.clone.1), dimensions={0}, to_apply=%region_3.4 | reduce | flops 393216 | bytes 1310722 | tf_op jit(solution)/shard_map/reduce_sum | solution.py:447
  (96 shorter events, 46.7 us)
Async XLA Ops:
  0.6 9.6 %collective-permute-start = (bf16[64,2048]{1,0:T(8,128)(2,1)}, bf16[64,2048]{1,0:T(8,128)(2,1)S(1)}, u32[]{:S(2)}, u32[]{:S(2)}) collective-permute-start(bf16[64,2048]{1,0:T(8,128)(2,1)} %refs_0_.1), channel_id=1, source_target_pairs={{0,1},{1,2},{2,3},{3,0},{4,5},{5,6},{6,7},{7,4},{8,9},{9,10},{10,1... | collective-permute-start | bytes 786440 | tf_op jit(solution)/shard_map/ppermute | solution.py:322
  2.3 13.1 %collective-permute-start.1 = (bf16[64,2048]{1,0:T(8,128)(2,1)}, bf16[64,2048]{1,0:T(8,128)(2,1)S(1)}, u32[]{:S(2)}, u32[]{:S(2)}) collective-permute-start(bf16[64,2048]{1,0:T(8,128)(2,1)} %refs_0_.1), channel_id=1, source_target_pairs={{0,3},{1,0},{2,1},{3,2},{4,7},{5,4},{6,5},{7,6},{8,11},{9,8},{10,9... | collective-permute-start | bytes 786440 | tf_op jit(solution)/shard_map/ppermute | solution.py:322
  4.0 13.1 %collective-permute-start.2 = (bf16[64,2048]{1,0:T(8,128)(2,1)}, bf16[64,2048]{1,0:T(8,128)(2,1)S(1)}, u32[]{:S(2)}, u32[]{:S(2)}) collective-permute-start(bf16[64,2048]{1,0:T(8,128)(2,1)} %refs_0_.1), channel_id=1, source_target_pairs={{0,2},{1,3},{2,0},{3,1},{4,6},{5,7},{6,4},{7,5},{8,10},{9,11},{10,... | collective-permute-start | bytes 786440 | tf_op jit(solution)/shard_map/ppermute | solution.py:322
  24.3 10.2 %collective-permute-start.3 = (bf16[2,128,256]{2,1,0:T(8,128)(2,1)S(1)}, bf16[2,128,256]{2,1,0:T(8,128)(2,1)}, u32[]{:S(2)}, u32[]{:S(2)}) collective-permute-start(bf16[2,128,256]{2,1,0:T(8,128)(2,1)S(1)} %pad_maximum_fusion.6), channel_id=1, source_target_pairs={{224,0},{228,4},{232,8},{236,12},{240,16},{244,20},{248,24},{252,2... | collective-permute-start | bytes 393224 | tf_op jit(solution)/shard_map/ppermute | solution.py:361
  26.7 11.2 %collective-permute-start.5 = (bf16[512,128]{1,0:T(8,128)(2,1)S(1)}, bf16[512,128]{1,0:T(8,128)(2,1)S(1)}, u32[]{:S(2)}, u32[]{:S(2)}) collective-permute-start(bf16[512,128]{1,0:T(8,128)(2,1)S(1)} %get-tuple-element.47.own_ref), channel_id=1, source_target_pairs={{0,8},{4,12},{8,16},{12,20},{16,24},{20,28},{24,0},{28,4},{32,40},... | collective-permute-start | bytes 393224 | tf_op jit(solution)/shard_map/ppermute | solution.py:27
  28.3 9.7 %collective-permute-start.6 = (bf16[512,128]{1,0:T(8,128)(2,1)S(1)}, bf16[512,128]{1,0:T(8,128)(2,1)S(1)}, u32[]{:S(2)}, u32[]{:S(2)}) collective-permute-start(bf16[512,128]{1,0:T(8,128)(2,1)S(1)} %get-tuple-element.47.own_ref), channel_id=1, source_target_pairs={{0,24},{4,28},{8,0},{12,4},{16,8},{20,12},{24,16},{28,20},{32,56},... | collective-permute-start | bytes 393224 | tf_op jit(solution)/shard_map/ppermute | solution.py:27
  28.8 9.2 %collective-permute-start.7 = (bf16[512,128]{1,0:T(8,128)(2,1)S(1)}, bf16[512,128]{1,0:T(8,128)(2,1)S(1)}, u32[]{:S(2)}, u32[]{:S(2)}) collective-permute-start(bf16[512,128]{1,0:T(8,128)(2,1)S(1)} %get-tuple-element.47.own_ref), channel_id=1, source_target_pairs={{0,16},{4,20},{8,24},{12,28},{16,0},{20,4},{24,8},{28,12},{32,48},... | collective-permute-start | bytes 393224 | tf_op jit(solution)/shard_map/ppermute | solution.py:27
  31.0 27.7 %collective-permute-start.8 = (bf16[4,128,256]{2,1,0:T(8,128)(2,1)S(1)}, bf16[4,128,256]{2,1,0:T(8,128)(2,1)S(1)}, u32[]{:S(2)}, u32[]{:S(2)}) collective-permute-start(bf16[4,128,256]{2,1,0:T(8,128)(2,1)S(1)} %bitcast.61), channel_id=1, source_target_pairs={{0,4},{4,0},{8,12},{12,8},{16,20},{20,16},{24,28},{28,24},{32,36},... | collective-permute-start | bytes 786440 | tf_op jit(solution)/shard_map/ppermute | solution.py:27
  36.0 6.7 %collective-permute-start.4 = (bf16[30,512]{1,0:T(8,128)(2,1)S(1)}, bf16[30,512]{1,0:T(8,128)(2,1)S(1)}, u32[]{:S(2)}, u32[]{:S(2)}) collective-permute-start(bf16[30,512]{1,0:T(8,128)(2,1)S(1)} %slice.345), channel_id=1, source_target_pairs={{0,4},{4,8},{8,12},{12,16},{16,20},{20,24},{24,28},{28,32},{32,36}... | collective-permute-start | bytes 92168 | tf_op jit(solution)/shard_map/ppermute | solution.py:37
  38.8 16.5 %collective-permute-start.10 = (bf16[2048,128]{1,0:T(8,128)(2,1)}, bf16[2048,128]{1,0:T(8,128)(2,1)}, u32[]{:S(2)}, u32[]{:S(2)}) collective-permute-start(bf16[2048,128]{1,0:T(8,128)(2,1)} %pad_maximum_fusion.1), channel_id=1, source_target_pairs={{0,32},{4,36},{8,40},{12,44},{16,48},{20,52},{24,56},{28,60},{32,6... | collective-permute-start | bytes 1572872 | tf_op jit(solution)/shard_map/ppermute | solution.py:27
  40.5 14.8 %collective-permute-start.11 = (bf16[2048,128]{1,0:T(8,128)(2,1)}, bf16[2048,128]{1,0:T(8,128)(2,1)}, u32[]{:S(2)}, u32[]{:S(2)}) collective-permute-start(bf16[2048,128]{1,0:T(8,128)(2,1)} %pad_maximum_fusion.1), channel_id=1, source_target_pairs={{0,224},{4,228},{8,232},{12,236},{16,240},{20,244},{24,248},{28,25... | collective-permute-start | bytes 1572872 | tf_op jit(solution)/shard_map/ppermute | solution.py:27
  41.4 17.2 %collective-permute-start.9 = (bf16[2,128,256]{2,1,0:T(8,128)(2,1)}, bf16[2,128,256]{2,1,0:T(8,128)(2,1)}, u32[]{:S(2)}, u32[]{:S(2)}) collective-permute-start(bf16[2,128,256]{2,1,0:T(8,128)(2,1)} %collective-permute-done.3), channel_id=1, source_target_pairs={{0,4},{4,0},{8,12},{12,8},{16,20},{20,16},{24,28},{28,24},{32,36},... | collective-permute-start | bytes 393224 | tf_op jit(solution)/shard_map/ppermute | solution.py:27
  46.7 8.5 %all-to-all-start = ((f32[4,1,512]{2,1,0:T(1,128)}), f32[4,1,512]{2,1,0:T(1,128)S(1)}, u32[]{:S(2)}, u32[]{:S(2)}) async-start(f32[4,1,512]{2,1,0:T(1,128)} %broadcast_in_dim.7), calls=%async_computation | async-start | bytes 16384 | tf_op jit(solution)/shard_map/all_to_all | solution.py:42
  55.3 14.6 %collective-permute-start.12 = (bf16[2048,128]{1,0:T(8,128)(2,1)}, bf16[2048,128]{1,0:T(8,128)(2,1)S(1)}, u32[]{:S(2)}, u32[]{:S(2)}) collective-permute-start(bf16[2048,128]{1,0:T(8,128)(2,1)} %collective-permute-done.10.a_ref), channel_id=1, source_target_pairs={{0,32},{4,36},{8,40},{12,44},{16,48},{20,52},{24,56},{28,60},{32,6... | collective-permute-start | bytes 1572872 | tf_op jit(solution)/shard_map/ppermute | solution.py:27
  56.4 14.4 %collective-permute-start.13 = (bf16[2048,128]{1,0:T(8,128)(2,1)}, bf16[2048,128]{1,0:T(8,128)(2,1)S(1)}, u32[]{:S(2)}, u32[]{:S(2)}) collective-permute-start(bf16[2048,128]{1,0:T(8,128)(2,1)} %collective-permute-done.11.b_ref), channel_id=1, source_target_pairs={{0,224},{4,228},{8,232},{12,236},{16,240},{20,244},{24,248},{28,25... | collective-permute-start | bytes 1572872 | tf_op jit(solution)/shard_map/ppermute | solution.py:27
  70.8 14.4 %collective-permute-start.14 = (bf16[2048,128]{1,0:T(8,128)(2,1)S(1)}, bf16[2048,128]{1,0:T(8,128)(2,1)S(1)}, u32[]{:S(2)}, u32[]{:S(2)}) collective-permute-start(bf16[2048,128]{1,0:T(8,128)(2,1)S(1)} %collective-permute-done.12.a_ref), channel_id=1, source_target_pairs={{0,32},{4,36},{8,40},{12,44},{16,48},{20,52},{24,56},{28,60},{32,6... | collective-permute-start | bytes 1572872 | tf_op jit(solution)/shard_map/ppermute | solution.py:27
  72.5 13.0 %collective-permute-start.15 = (bf16[2048,128]{1,0:T(8,128)(2,1)S(1)}, bf16[2048,128]{1,0:T(8,128)(2,1)S(1)}, u32[]{:S(2)}, u32[]{:S(2)}) collective-permute-start(bf16[2048,128]{1,0:T(8,128)(2,1)S(1)} %collective-permute-done.13.b_ref), channel_id=1, source_target_pairs={{0,224},{4,228},{8,232},{12,236},{16,240},{20,244},{24,248},{28,25... | collective-permute-start | bytes 1572872 | tf_op jit(solution)/shard_map/ppermute | solution.py:27
  85.6 6.5 %collective-permute-start.16 = (bf16[1024,128]{1,0:T(8,128)(2,1)S(1)}, bf16[1024,128]{1,0:T(8,128)(2,1)S(1)}, u32[]{:S(2)}, u32[]{:S(2)}) collective-permute-start(bf16[1024,128]{1,0:T(8,128)(2,1)S(1)} %slice.327), channel_id=1, source_target_pairs={{0,32},{4,36},{8,40},{12,44},{16,48},{20,52},{24,56},{28,60},{32,6... | collective-permute-start | bytes 786440 | tf_op jit(solution)/shard_map/ppermute | solution.py:27
  87.4 6.4 %collective-permute-start.17 = (bf16[1024,128]{1,0:T(8,128)(2,1)S(1)}, bf16[1024,128]{1,0:T(8,128)(2,1)S(1)}, u32[]{:S(2)}, u32[]{:S(2)}) collective-permute-start(bf16[1024,128]{1,0:T(8,128)(2,1)S(1)} %slice.328), channel_id=1, source_target_pairs={{0,224},{4,228},{8,232},{12,236},{16,240},{20,244},{24,248},{28,25... | collective-permute-start | bytes 786440 | tf_op jit(solution)/shard_map/ppermute | solution.py:27
  102.8 3.8 %collective-permute-start.19 = (f32[12,128,256]{2,1,0:T(8,128)}, f32[12,128,256]{2,1,0:T(8,128)}, u32[]{:S(2)}, u32[]{:S(2)}) collective-permute-start(f32[12,128,256]{2,1,0:T(8,128)} %get-tuple-element.85), channel_id=1, source_target_pairs={{0,4},{4,0},{8,12},{12,8},{16,20},{20,16},{24,28},{28,24},{32,36},... | collective-permute-start | bytes 4718600 | tf_op jit(solution)/shard_map/ppermute | solution.py:27
  102.8 3.8 %collective-permute-start.18 = (f32[12,8,256]{2,1,0:T(8,128)S(1)}, f32[12,8,256]{2,1,0:T(8,128)S(1)}, u32[]{:S(2)}, u32[]{:S(2)}) collective-permute-start(f32[12,8,256]{2,1,0:T(8,128)S(1)} %get-tuple-element.84), channel_id=1, source_target_pairs={{0,4},{4,0},{8,12},{12,8},{16,20},{20,16},{24,28},{28,24},{32,36},... | collective-permute-start | bytes 294920 | tf_op jit(solution)/shard_map/ppermute | solution.py:27
  109.9 18.5 %collective-permute-start.20 = (bf16[2,128,256]{2,1,0:T(8,128)(2,1)S(1)}, bf16[2,128,256]{2,1,0:T(8,128)(2,1)S(1)}, u32[]{:S(2)}, u32[]{:S(2)}) collective-permute-start(bf16[2,128,256]{2,1,0:T(8,128)(2,1)S(1)} %get-tuple-element.96), channel_id=1, source_target_pairs={{0,224},{4,228},{8,232},{12,236},{16,240},{20,244},{24,248},{28,25... | collective-permute-start | bytes 393224 | tf_op jit(solution)/shard_map/ppermute | solution.py:430
  132.4 19.1 %all-to-all-start.1 = ((bf16[4,64,2048]{2,1,0:T(8,128)(2,1)}), bf16[4,64,2048]{2,1,0:T(8,128)(2,1)}, u32[]{:S(2)}, u32[]{:S(2)}) async-start(bf16[4,64,2048]{2,1,0:T(8,128)(2,1)} %bitcast.45), calls=%async_computation.1 | async-start | bytes 2097152 | tf_op jit(solution)/shard_map/all_to_all | solution.py:446
  136.7 8.7 %collective-permute-start.21 = (f32[2,2,256]{2,0,1:T(2,128)S(1)}, f32[2,2,256]{2,0,1:T(2,128)S(1)}, u32[]{:S(2)}, u32[]{:S(2)}) collective-permute-start(f32[2,2,256]{2,0,1:T(2,128)S(1)} %copy.42), channel_id=1, source_target_pairs={{0,224},{4,228},{8,232},{12,236},{16,240},{20,244},{24,248},{28,25... | collective-permute-start | bytes 12296 | tf_op jit(solution)/shard_map/ppermute | solution.py:431
  (15 other events, 152.9 us)

commit v4 on v3

--- a/solution.py
+++ b/solution.py
@@ -227,25 +227,23 @@
     )
 
 
-def front_kernel(where_ref, *refs):
-    (left_ref, right_ref, far_ref, normed_ref, kv_ref), held = refs[5:10], refs[10:15]
-    own_ref, gain_ref, wk_ref, wv_ref, key_gain_ref = held
-    copies = [pltpu.make_async_copy(refs[k], held[k], refs[15].at[k]) for k in range(5)]
-    for k in (1, 0, 2, 3, 4):
-        copies[k].start()
+def stage_kernel(*refs):
+    for before, after in zip(refs[:5], refs[5:]):
+        after[...] = before[...]
+
+
+def front_kernel(
+    where_ref, own_ref, gain_ref, wk_ref, wv_ref, key_gain_ref, left_ref, right_ref, far_ref,
+    normed_ref, kv_ref
+):
     t = where_ref[3]
-    copies[1].wait()
     for ref, step in ((left_ref, 3), (right_ref, 1), (far_ref, 2), (own_ref, 0)):
-        if step == 0:
-            copies[0].wait()
         row = pl.multiple_of(lax.rem(t + step, 4) * 64, 64)
         rows = ref[...].astype(jnp.float32)
         mean = jnp.mean(rows * rows, axis=1, keepdims=True)
         normed_ref[pl.ds(row, 64), :] = (rows * lax.rsqrt(mean + 1e-06) * gain_ref[...]).astype(
             jnp.bfloat16
         )
-    for k in (2, 3, 4):
-        copies[k].wait()
     normed = normed_ref[...]
     keys = jnp.dot(normed, wk_ref[...], preferred_element_type=jnp.float32)
     first = lax.broadcasted_iota(jnp.int32, keys.shape, 1) < 64
@@ -321,31 +319,22 @@
     rows_of = [
         lax.ppermute(tokens, "tp", [(t, (t + step) % 4) for t in range(4)]) for step in (2, 1, 3)
     ]
+    staged = (tokens, norm_gain[None], w_key, w_value, key_gain)
+    staged = plain_kernel(
+        stage_kernel, "stage", staged, tuple(pltpu.VMEM(a.shape, a.dtype) for a in staged), smem=0
+    )
     normed_shape = jax.ShapeDtypeStruct((tok_dev, tokens.shape[1]), jnp.bfloat16)
     rows_block, own = plain_kernel(
         front_kernel,
         "front",
         (
             where,
-            tokens,
-            norm_gain[None],
-            w_key,
-            w_value,
-            key_gain,
+            *staged,
             rows_of[1],
             rows_of[2],
             rows_of[0],
         ),
         (normed_shape, jax.ShapeDtypeStruct((512, 128), jnp.bfloat16)),
-        scratch=[
-            pltpu.VMEM(tokens.shape, jnp.bfloat16),
-            pltpu.VMEM((1, tokens.shape[1]), jnp.float32),
-            pltpu.VMEM(w_key.shape, jnp.bfloat16),
-            pltpu.VMEM(w_value.shape, jnp.bfloat16),
-            pltpu.VMEM(key_gain.shape, jnp.float32),
-            pltpu.SemaphoreType.DMA((5,)),
-        ],
-        hbm=5,
     )
 
     query_t = plain_kernel(
@@ -363,11 +352,11 @@
     left = sp_send(own, lambda z, x, c: (z, x + 1, c))
     right = sp_send(own, lambda z, x, c: (z, x - 1, c))
     far = sp_send(own, lambda z, x, c: (z, x + 2, c))
-    guest_early, rows_block = lax.optimization_barrier((guest, rows_block))
     glu_a = jnp.dot(rows_block, w_glu_a, preferred_element_type=jnp.float32)
     glu_b = jnp.dot(rows_block, w_glu_b, preferred_element_type=jnp.float32)
     gated_rows = (glu_a * jax.nn.sigmoid(glu_b)).astype(jnp.bfloat16)
     prev_rows = shifted(gated_rows[tok_dev - (KW - 1) :], "sp", 1)
+    guest_early, gated_rows = lax.optimization_barrier((guest, gated_rows))
     partner_guest = sp_send(guest_early, swap)
     mine = jnp.concatenate([query_t, guest_early], axis=0).reshape(-1, head_dim, tok_dev)
     other = jnp.concatenate([partner_q, partner_guest], axis=0).reshape(-1, head_dim, tok_dev)

time: 155 us -> 155 us (level)
  waiting for transfers between devices: 35.9 us -> 31.9 us
  starting transfers between devices: 55.6 us -> 58.3 us
    ppermute x3, waiting for transfers between devices: 9.1 us -> 3.5 us  [on_device(): lax.ppermute(tokens, 'tp', [(t, (t + step) % 4) for t in range(4)])]
    ppermute x1, waiting for transfers between devices: 3.54 us -> 7.67 us  [on_device(): guest = lax.ppermute(given, 'sp', mirrored((7, 6, 5)))]
    ppermute x15, waiting for transfers between devices: 9.1 us -> 6.68 us  [sp_send(): return lax.ppermute(value, 'sp', sp_table(move))]
    ppermute x1, starting transfers between devices: 15.4 us -> 17.1 us  [on_device(): back_out = lax.ppermute(head_out[heads:], 'sp', mirrored((0, 1, 2)))]
    unnamed x30 -> x32, local copies, waits for them, and re-layouts: 7.01 us -> 8.44 us
    pallas_call x8 -> x9, Pallas kernels: 33.6 us -> 33.4 us  [plain_kernel(): pl.pallas_call(body, out_shape=out_shape, in_specs=[SMEM_SPEC] * smem + [...]
  transfers between devices with their start and end apart: 24 -> 24, of which waited for: 14 -> 13; matrix products, arithmetic and copies ran while one was open for 9% -> 9% of each run, Pallas kernels for 14% -> 14%
where the time goes in v4:
time: 155 us; the launch traced here: 154 us
  starting transfers between devices  58.3 us (38%)
  Pallas kernels  33.4 us (22%)
  waiting for transfers between devices  31.9 us (21%)
  local copies, waits for them, and re-layouts  12.3 us (8%)
  other arithmetic  9.11 us (6%)
  matrix products  7.66 us (5%)
    pallas_call x9, Pallas kernels, plain_kernel(): pl.pallas_call(body, out_shape=out_shape, in_specs=[SMEM_SPEC] * smem + [...  33.4 us
    ppermute x15, starting transfers between devices, sp_send(): return lax.ppermute(value, 'sp', sp_table(move))  17.8 us
    ppermute x1, starting transfers between devices, on_device(): back_out = lax.ppermute(head_out[heads:], 'sp', mirrored((0, 1, 2)))  17.1 us
    unnamed x32, local copies, waits for them, and re-layouts  8.44 us
    ppermute x1, waiting for transfers between devices, on_device(): guest = lax.ppermute(given, 'sp', mirrored((7, 6, 5)))  7.67 us
    ppermute x1, starting transfers between devices, on_device(): back_logs = lax.ppermute(logs[heads:], 'sp', mirrored((0, 1, 2)))  7.39 us
    ppermute x15, waiting for transfers between devices, sp_send(): return lax.ppermute(value, 'sp', sp_table(move))  6.68 us
    all_to_all x1, waiting for transfers between devices, on_device(): lax.all_to_all(out_part.reshape(tp_count, -1, out_part.shape[1]), 'tp', 0...  5.49 us
  transfers between devices with their start and end apart: 24, of which 13 were waited for; matrix products, arithmetic and copies ran while one was open for 9% of the time, Pallas kernels for 14%

profile of v4, /device:TPU:34, one launch (start us, length us, event | category | flops | bytes accessed | tf_op | source)
XLA Modules:
  0.0 153.6 jit_solution(383891081088735773)
XLA Ops:
  4.0 2.0 %collective-permute-start.2 = (bf16[64,2048]{1,0:T(8,128)(2,1)}, bf16[64,2048]{1,0:T(8,128)(2,1)S(1)}, u32[]{:S(2)}, u32[]{:S(2)}) collective-permute-start(bf16[64,2048]{1,0:T(8,128)(2,1)} %refs_0_.1), channel_id=1, source_target_pairs={{0,2},{1,3},{2,0},{3,1},{4,6},{5,7},{6,4},{7,5},{8,10},{9,11},{10,... | collective-permute-start | bytes 786440 | tf_op jit(solution)/shard_map/ppermute | solution.py:320
  20.8 2.1 %collective-permute-start.6 = (bf16[512,128]{1,0:T(8,128)(2,1)S(1)}, bf16[512,128]{1,0:T(8,128)(2,1)S(1)}, u32[]{:S(2)}, u32[]{:S(2)}) collective-permute-start(bf16[512,128]{1,0:T(8,128)(2,1)S(1)} %get-tuple-element.56.own_ref), channel_id=1, source_target_pairs={{0,16},{4,20},{8,24},{12,28},{16,0},{20,4},{24,8},{28,12},{32,48},... | collective-permute-start | bytes 393224 | tf_op jit(solution)/shard_map/ppermute | solution.py:27
  31.6 7.7 %collective-permute-done.7 = bf16[2,128,256]{2,1,0:T(8,128)(2,1)S(1)} collective-permute-done((bf16[2,128,256]{2,1,0:T(8,128)(2,1)S(1)}, bf16[2,128,256]{2,1,0:T(8,128)(2,1)S(1)}, u32[]{:S(2)}, u32[]{:S(2)}) %collective-permute-start.7) | collective-permute-done | bytes 131104 | tf_op jit(solution)/shard_map/ppermute | solution.py:350
  42.7 3.4 %fusion.40 = (f32[256]{0:T(256)S(1)}, f32[256]{0:T(256)S(1)}, f32[256,512]{1,0:T(8,128)}) fusion(bf16[256,512]{1,0:T(8,128)(2,1)S(1)} %fusion.4, f32[512]{0:T(512)S(1)} %bitcast.78, bf16[30,512]{1,0:T(8,128)(2,1)S(1)} %collective-permute-done.3, f32[512]{0:T(512)S(1)} %bitcast.79, f32[512]{0:T(512)S(1)} %bitcast.81, f32[512]{0:T(512)S(1)} %bitcast.82, ...), kind=kLoop, calls=%fused_computation.103 | loop fusion | flops 24247808 | bytes 882688 | tf_op jit(solution)/shard_map/reduce_sum | solution.py:377
  46.7 3.2 %all-to-all-start = ((f32[4,1,512]{2,1,0:T(1,128)}), f32[4,1,512]{2,1,0:T(1,128)S(1)}, u32[]{:S(2)}, u32[]{:S(2)}) async-start(f32[4,1,512]{2,1,0:T(1,128)} %broadcast_in_dim.7), calls=%async_computation | async-start | bytes 16384 | tf_op jit(solution)/shard_map/all_to_all | solution.py:42
  51.0 4.2 %all-to-all-done = f32[4,1,512]{2,1,0:T(1,128)S(1)} async-done(((f32[4,1,512]{2,1,0:T(1,128)}), f32[4,1,512]{2,1,0:T(1,128)S(1)}, u32[]{:S(2)}, u32[]{:S(2)}) %all-to-all-start) | async-done | bytes 8224 | tf_op jit(solution)/shard_map/all_to_all | solution.py:42
  56.6 2.3 %collective-permute-start.13 = (bf16[2048,128]{1,0:T(8,128)(2,1)}, bf16[2048,128]{1,0:T(8,128)(2,1)S(1)}, u32[]{:S(2)}, u32[]{:S(2)}) collective-permute-start(bf16[2048,128]{1,0:T(8,128)(2,1)} %collective-permute-done.11.b_ref), channel_id=1, source_target_pairs={{0,224},{4,228},{8,232},{12,236},{16,240},{20,244},{24,248},{28,25... | collective-permute-start | bytes 1572872 | tf_op jit(solution)/shard_map/ppermute | solution.py:27
  60.0 8.9 %attend_0.1 = (f32[12,8,256]{2,1,0:T(8,128)S(1)}, f32[12,8,256]{2,1,0:T(8,128)S(1)}, f32[12,128,256]{2,1,0:T(8,128)S(1)}, f32[12,128,256]{2,1,0:T(8,128)S(1)}, bf16[24,256,256]{2,1,0:T(8,128)(2,1)S(1)}) custom-call(s32[4]{0:T(128)S(1)} %pad_add_fusion.where_ref, bf16[24,64,256]{2,1,0:T(8,128)(2,1)S(1)} %bitcast.63, ...), custom_call_target="tpu_custom_call" | custom-call | flops 1610612736 | bytes 2097152 | tf_op jit(solution)/shard_map/attend_0/pallas_call | solution.py:193
  70.1 3.5 %collective-permute-start.15 = (bf16[2048,128]{1,0:T(8,128)(2,1)S(1)}, bf16[2048,128]{1,0:T(8,128)(2,1)S(1)}, u32[]{:S(2)}, u32[]{:S(2)}) collective-permute-start(bf16[2048,128]{1,0:T(8,128)(2,1)S(1)} %collective-permute-done.13.b_ref), channel_id=1, source_target_pairs={{0,224},{4,228},{8,232},{12,236},{16,240},{20,244},{24,248},{28,25... | collective-permute-start | bytes 1572872 | tf_op jit(solution)/shard_map/ppermute | solution.py:27
  73.7 2.2 %fusion.5 = f32[256,2048]{1,0:T(8,128)} fusion(bf16[512,2048]{1,0:T(8,128)(2,1)S(1)} %copy-done, f32[256,512]{1,0:T(8,128)S(1)} %copy-done.11, f32[512]{0:T(512)S(1)} %copy-done.15, f32[256]{0:T(256)S(1)} %get-tuple-element.143, f32[256]{0:T(256)S(1)} %get-tuple-element.142), kind=kOutput, calls=%fused_computation.44 | convolution fusion | flops 537919488 | bytes 4722688 | tf_op jit(solution)/shard_map/dot_general | solution.py:385
  75.9 9.6 %attend_1.1 = (f32[12,8,256]{2,1,0:T(8,128)S(1)}, f32[12,8,256]{2,1,0:T(8,128)S(1)}, f32[12,128,256]{2,1,0:T(8,128)S(1)}, f32[12,128,256]{2,1,0:T(8,128)S(1)}) custom-call(s32[4]{0:T(128)S(1)} %pad_add_fusion.where_ref, bf16[24,256,256]{2,1,0:T(8,128)(2,1)S(1)} %get-tuple-element.63.q_ref, ...), custom_call_target="tpu_custom_call", output_to_operand_aliasing={{0}: (4, {}), {1}: (5, {}), {2}: (6, {}), {3}: (7, {})} | custom-call | flops 3221225472 | bytes 2097152 | tf_op jit(solution)/shard_map/attend_1/pallas_call | solution.py:193
  85.6 2.1 %collective-permute-start.17 = (bf16[1024,128]{1,0:T(8,128)(2,1)S(1)}, bf16[1024,128]{1,0:T(8,128)(2,1)S(1)}, u32[]{:S(2)}, u32[]{:S(2)}) collective-permute-start(bf16[1024,128]{1,0:T(8,128)(2,1)S(1)} %slice.328), channel_id=1, source_target_pairs={{0,224},{4,228},{8,232},{12,236},{16,240},{20,244},{24,248},{28,25... | collective-permute-start | bytes 786440 | tf_op jit(solution)/shard_map/ppermute | solution.py:27
  87.7 2.7 %attend_2.1 = (f32[12,8,256]{2,1,0:T(8,128)S(1)}, f32[12,8,256]{2,1,0:T(8,128)S(1)}, f32[12,128,256]{2,1,0:T(8,128)S(1)}, f32[12,128,256]{2,1,0:T(8,128)S(1)}) custom-call(s32[4]{0:T(128)S(1)} %pad_add_fusion.where_ref, bf16[24,256,256]{2,1,0:T(8,128)(2,1)S(1)} %get-tuple-element.63.q_ref, ...), custom_call_target="tpu_custom_call", output_to_operand_aliasing={{0}: (4, {}), {1}: (5, {}), {2}: (6, {}), {3}: (7, {})} | custom-call | flops 3221225472 | bytes 2097152 | tf_op jit(solution)/shard_map/attend_2/pallas_call | solution.py:193
  92.1 4.1 %attend_3.1 = (f32[12,8,256]{2,1,0:T(8,128)S(1)}, f32[12,8,256]{2,1,0:T(8,128)S(1)}, f32[12,128,256]{2,1,0:T(8,128)S(1)}, f32[12,128,256]{2,1,0:T(8,128)S(1)}) custom-call(s32[4]{0:T(128)S(1)} %pad_add_fusion.where_ref, bf16[24,256,256]{2,1,0:T(8,128)(2,1)S(1)} %get-tuple-element.63.q_ref, ...), custom_call_target="tpu_custom_call", output_to_operand_aliasing={{0}: (4, {}), {1}: (5, {}), {2}: (6, {}), {3}: (7, {})} | custom-call | flops 3221225472 | bytes 2097152 | tf_op jit(solution)/shard_map/attend_3/pallas_call | solution.py:193
  96.3 3.6 %attend_4.1 = (f32[12,8,256]{2,1,0:T(8,128)S(1)}, f32[12,8,256]{2,1,0:T(8,128)S(1)}, f32[12,128,256]{2,1,0:T(8,128)S(1)}, f32[12,128,256]{2,1,0:T(8,128)}) custom-call(s32[4]{0:T(128)S(1)} %pad_add_fusion.where_ref, bf16[24,256,256]{2,1,0:T(8,128)(2,1)S(1)} %get-tuple-element.63.q_ref, bf16[1024,128]{1,0:T(8,128)(2,1)S(1)} %collective-permute-done.16.a_ref, ...), custom_call_target="tpu_custom_call" | custom-call | flops 1610612736 | bytes 2097152 | tf_op jit(solution)/shard_map/attend_4/pallas_call | solution.py:193
  101.7 3.1 %collective-permute-done.18.stats_b = f32[12,8,256]{2,1,0:T(8,128)S(1)} collective-permute-done((f32[12,8,256]{2,1,0:T(8,128)S(1)}, f32[12,8,256]{2,1,0:T(8,128)S(1)}, u32[]{:S(2)}, u32[]{:S(2)}) %collective-permute-start.18) | collective-permute-done | bytes 98336 | tf_op jit(solution)/shard_map/ppermute | solution.py:27
  106.2 1.9 %finish.1 = (bf16[6,128,256]{2,1,0:T(8,128)(2,1)S(1)}, f32[12,8,256]{2,1,0:T(8,128)S(1)}) custom-call(f32[4]{0:T(128)S(1)} %copy-done.9, f32[128,1]{1,0:T(8,128)S(1)} %copy.41.gain_ref, f32[12,8,256]{2,1,0:T(8,128)S(1)} %get-tuple-element.92.stats_a, f32[12,128,256]{2,1,0:T(8,128)S(1)} %copy-done.3, f32[12,8,256]{2,1,0:T(8,128)S(1)} %collective-permute-done.18.stats_b, ...), custom_call_target="tpu_custom_call" | custom-call | flops 268435456 | bytes 2097152 | tf_op jit(solution)/shard_map/finish/pallas_call | solution.py:193
  108.2 17.1 %collective-permute-start.20 = (bf16[2,128,256]{2,1,0:T(8,128)(2,1)S(1)}, bf16[2,128,256]{2,1,0:T(8,128)(2,1)S(1)}, u32[]{:S(2)}, u32[]{:S(2)}) collective-permute-start(bf16[2,128,256]{2,1,0:T(8,128)(2,1)S(1)} %get-tuple-element.106), channel_id=1, source_target_pairs={{0,224},{4,228},{8,232},{12,236},{16,240},{20,244},{24,248},{28,25... | collective-permute-start | bytes 393224 | tf_op jit(solution)/shard_map/ppermute | solution.py:419
  125.3 3.0 %collective-permute-done.20 = bf16[2,128,256]{2,1,0:T(8,128)(2,1)S(1)} collective-permute-done((bf16[2,128,256]{2,1,0:T(8,128)(2,1)S(1)}, bf16[2,128,256]{2,1,0:T(8,128)(2,1)S(1)}, u32[]{:S(2)}, u32[]{:S(2)}) %collective-permute-start.20) | collective-permute-done | bytes 131104 | tf_op jit(solution)/shard_map/ppermute | solution.py:419
  128.4 3.9 %fusion = bf16[256,2048]{1,0:T(8,128)(2,1)} fusion(f32[256,2048]{1,0:T(8,128)} %fusion.5, bf16[512,256]{1,0:T(8,128)(2,1)S(1)} %bitcast.67, bf16[512,2048]{1,0:T(8,128)(2,1)} %param.29), kind=kOutput, calls=%fused_computation.30 | convolution fusion | flops 537919488 | bytes 5505024 | tf_op jit(solution)/shard_map/dot_general | solution.py:431
  132.3 4.2 %all-to-all-start.1 = ((bf16[4,64,2048]{2,1,0:T(8,128)(2,1)}), bf16[4,64,2048]{2,1,0:T(8,128)(2,1)}, u32[]{:S(2)}, u32[]{:S(2)}) async-start(bf16[4,64,2048]{2,1,0:T(8,128)(2,1)} %bitcast.45), calls=%async_computation.1 | async-start | bytes 2097152 | tf_op jit(solution)/shard_map/all_to_all | solution.py:435
  136.6 7.4 %collective-permute-start.21 = (f32[2,2,256]{2,0,1:T(2,128)S(1)}, f32[2,2,256]{2,0,1:T(2,128)S(1)}, u32[]{:S(2)}, u32[]{:S(2)}) collective-permute-start(f32[2,2,256]{2,0,1:T(2,128)S(1)} %copy.42), channel_id=1, source_target_pairs={{0,224},{4,228},{8,232},{12,236},{16,240},{20,244},{24,248},{28,25... | collective-permute-start | bytes 12296 | tf_op jit(solution)/shard_map/ppermute | solution.py:420
  146.0 5.5 %all-to-all-done.1 = bf16[4,64,2048]{2,1,0:T(8,128)(2,1)} async-done(((bf16[4,64,2048]{2,1,0:T(8,128)(2,1)}), bf16[4,64,2048]{2,1,0:T(8,128)(2,1)}, u32[]{:S(2)}, u32[]{:S(2)}) %all-to-all-start.1) | async-done | bytes 1048608 | tf_op jit(solution)/shard_map/all_to_all | solution.py:435
  151.5 2.2 %reduce_sum.42 = bf16[64,2048]{1,0:T(8,128)(2,1)} reduce(bf16[4,64,2048]{2,1,0:T(8,128)(2,1)} %all-to-all-done.1, bf16[]{:T(256)} %constant.69.clone.1), dimensions={0}, to_apply=%region_3.4 | reduce | flops 393216 | bytes 1310722 | tf_op jit(solution)/shard_map/reduce_sum | solution.py:436
  (99 shorter events, 42.7 us)
Async XLA Ops:
  0.6 12.9 %collective-permute-start = (bf16[64,2048]{1,0:T(8,128)(2,1)}, bf16[64,2048]{1,0:T(8,128)(2,1)S(1)}, u32[]{:S(2)}, u32[]{:S(2)}) collective-permute-start(bf16[64,2048]{1,0:T(8,128)(2,1)} %refs_0_.1), channel_id=1, source_target_pairs={{0,1},{1,2},{2,3},{3,0},{4,5},{5,6},{6,7},{7,4},{8,9},{9,10},{10,1... | collective-permute-start | bytes 786440 | tf_op jit(solution)/shard_map/ppermute | solution.py:320
  2.3 13.1 %collective-permute-start.1 = (bf16[64,2048]{1,0:T(8,128)(2,1)}, bf16[64,2048]{1,0:T(8,128)(2,1)S(1)}, u32[]{:S(2)}, u32[]{:S(2)}) collective-permute-start(bf16[64,2048]{1,0:T(8,128)(2,1)} %refs_0_.1), channel_id=1, source_target_pairs={{0,3},{1,0},{2,1},{3,2},{4,7},{5,4},{6,5},{7,6},{8,11},{9,8},{10,9... | collective-permute-start | bytes 786440 | tf_op jit(solution)/shard_map/ppermute | solution.py:320
  4.0 13.1 %collective-permute-start.2 = (bf16[64,2048]{1,0:T(8,128)(2,1)}, bf16[64,2048]{1,0:T(8,128)(2,1)S(1)}, u32[]{:S(2)}, u32[]{:S(2)}) collective-permute-start(bf16[64,2048]{1,0:T(8,128)(2,1)} %refs_0_.1), channel_id=1, source_target_pairs={{0,2},{1,3},{2,0},{3,1},{4,6},{5,7},{6,4},{7,5},{8,10},{9,11},{10,... | collective-permute-start | bytes 786440 | tf_op jit(solution)/shard_map/ppermute | solution.py:320
  18.7 10.7 %collective-permute-start.4 = (bf16[512,128]{1,0:T(8,128)(2,1)S(1)}, bf16[512,128]{1,0:T(8,128)(2,1)S(1)}, u32[]{:S(2)}, u32[]{:S(2)}) collective-permute-start(bf16[512,128]{1,0:T(8,128)(2,1)S(1)} %get-tuple-element.56.own_ref), channel_id=1, source_target_pairs={{0,8},{4,12},{8,16},{12,20},{16,24},{20,28},{24,0},{28,4},{32,40},... | collective-permute-start | bytes 393224 | tf_op jit(solution)/shard_map/ppermute | solution.py:27
  20.3 10.4 %collective-permute-start.5 = (bf16[512,128]{1,0:T(8,128)(2,1)S(1)}, bf16[512,128]{1,0:T(8,128)(2,1)S(1)}, u32[]{:S(2)}, u32[]{:S(2)}) collective-permute-start(bf16[512,128]{1,0:T(8,128)(2,1)S(1)} %get-tuple-element.56.own_ref), channel_id=1, source_target_pairs={{0,24},{4,28},{8,0},{12,4},{16,8},{20,12},{24,16},{28,20},{32,56},... | collective-permute-start | bytes 393224 | tf_op jit(solution)/shard_map/ppermute | solution.py:27
  20.8 9.9 %collective-permute-start.6 = (bf16[512,128]{1,0:T(8,128)(2,1)S(1)}, bf16[512,128]{1,0:T(8,128)(2,1)S(1)}, u32[]{:S(2)}, u32[]{:S(2)}) collective-permute-start(bf16[512,128]{1,0:T(8,128)(2,1)S(1)} %get-tuple-element.56.own_ref), channel_id=1, source_target_pairs={{0,16},{4,20},{8,24},{12,28},{16,0},{20,4},{24,8},{28,12},{32,48},... | collective-permute-start | bytes 393224 | tf_op jit(solution)/shard_map/ppermute | solution.py:27
  25.3 17.4 %collective-permute-start.3 = (bf16[30,512]{1,0:T(8,128)(2,1)S(1)}, bf16[30,512]{1,0:T(8,128)(2,1)S(1)}, u32[]{:S(2)}, u32[]{:S(2)}) collective-permute-start(bf16[30,512]{1,0:T(8,128)(2,1)S(1)} %slice.343), channel_id=1, source_target_pairs={{0,4},{4,8},{8,12},{12,16},{16,20},{20,24},{24,28},{28,32},{32,36}... | collective-permute-start | bytes 92168 | tf_op jit(solution)/shard_map/ppermute | solution.py:37
  28.2 11.1 %collective-permute-start.7 = (bf16[2,128,256]{2,1,0:T(8,128)(2,1)S(1)}, bf16[2,128,256]{2,1,0:T(8,128)(2,1)S(1)}, u32[]{:S(2)}, u32[]{:S(2)}) collective-permute-start(bf16[2,128,256]{2,1,0:T(8,128)(2,1)S(1)} %pad_maximum_fusion.6), channel_id=1, source_target_pairs={{224,0},{228,4},{232,8},{236,12},{240,16},{244,20},{248,24},{252,2... | collective-permute-start | bytes 393224 | tf_op jit(solution)/shard_map/ppermute | solution.py:350
  29.5 29.4 %collective-permute-start.8 = (bf16[4,128,256]{2,1,0:T(8,128)(2,1)S(1)}, bf16[4,128,256]{2,1,0:T(8,128)(2,1)S(1)}, u32[]{:S(2)}, u32[]{:S(2)}) collective-permute-start(bf16[4,128,256]{2,1,0:T(8,128)(2,1)S(1)} %bitcast.61), channel_id=1, source_target_pairs={{0,4},{4,0},{8,12},{12,8},{16,20},{20,16},{24,28},{28,24},{32,36},... | collective-permute-start | bytes 786440 | tf_op jit(solution)/shard_map/ppermute | solution.py:27
  39.9 15.6 %collective-permute-start.10 = (bf16[2048,128]{1,0:T(8,128)(2,1)}, bf16[2048,128]{1,0:T(8,128)(2,1)}, u32[]{:S(2)}, u32[]{:S(2)}) collective-permute-start(bf16[2048,128]{1,0:T(8,128)(2,1)} %pad_maximum_fusion.1), channel_id=1, source_target_pairs={{0,32},{4,36},{8,40},{12,44},{16,48},{20,52},{24,56},{28,60},{32,6... | collective-permute-start | bytes 1572872 | tf_op jit(solution)/shard_map/ppermute | solution.py:27
  41.8 14.0 %collective-permute-start.11 = (bf16[2048,128]{1,0:T(8,128)(2,1)}, bf16[2048,128]{1,0:T(8,128)(2,1)}, u32[]{:S(2)}, u32[]{:S(2)}) collective-permute-start(bf16[2048,128]{1,0:T(8,128)(2,1)} %pad_maximum_fusion.1), channel_id=1, source_target_pairs={{0,224},{4,228},{8,232},{12,236},{16,240},{20,244},{24,248},{28,25... | collective-permute-start | bytes 1572872 | tf_op jit(solution)/shard_map/ppermute | solution.py:27
  46.7 8.5 %all-to-all-start = ((f32[4,1,512]{2,1,0:T(1,128)}), f32[4,1,512]{2,1,0:T(1,128)S(1)}, u32[]{:S(2)}, u32[]{:S(2)}) async-start(f32[4,1,512]{2,1,0:T(1,128)} %broadcast_in_dim.7), calls=%async_computation | async-start | bytes 16384 | tf_op jit(solution)/shard_map/all_to_all | solution.py:42
  50.9 8.0 %collective-permute-start.9 = (bf16[2,128,256]{2,1,0:T(8,128)(2,1)}, bf16[2,128,256]{2,1,0:T(8,128)(2,1)}, u32[]{:S(2)}, u32[]{:S(2)}) collective-permute-start(bf16[2,128,256]{2,1,0:T(8,128)(2,1)} %copy-done.12), channel_id=1, source_target_pairs={{0,4},{4,0},{8,12},{12,8},{16,20},{20,16},{24,28},{28,24},{32,36},... | collective-permute-start | bytes 393224 | tf_op jit(solution)/shard_map/ppermute | solution.py:27
  55.8 14.4 %collective-permute-start.12 = (bf16[2048,128]{1,0:T(8,128)(2,1)}, bf16[2048,128]{1,0:T(8,128)(2,1)S(1)}, u32[]{:S(2)}, u32[]{:S(2)}) collective-permute-start(bf16[2048,128]{1,0:T(8,128)(2,1)} %collective-permute-done.10.a_ref), channel_id=1, source_target_pairs={{0,32},{4,36},{8,40},{12,44},{16,48},{20,52},{24,56},{28,60},{32,6... | collective-permute-start | bytes 1572872 | tf_op jit(solution)/shard_map/ppermute | solution.py:27
  56.6 13.5 %collective-permute-start.13 = (bf16[2048,128]{1,0:T(8,128)(2,1)}, bf16[2048,128]{1,0:T(8,128)(2,1)S(1)}, u32[]{:S(2)}, u32[]{:S(2)}) collective-permute-start(bf16[2048,128]{1,0:T(8,128)(2,1)} %collective-permute-done.11.b_ref), channel_id=1, source_target_pairs={{0,224},{4,228},{8,232},{12,236},{16,240},{20,244},{24,248},{28,25... | collective-permute-start | bytes 1572872 | tf_op jit(solution)/shard_map/ppermute | solution.py:27
  70.1 15.3 %collective-permute-start.14 = (bf16[2048,128]{1,0:T(8,128)(2,1)S(1)}, bf16[2048,128]{1,0:T(8,128)(2,1)S(1)}, u32[]{:S(2)}, u32[]{:S(2)}) collective-permute-start(bf16[2048,128]{1,0:T(8,128)(2,1)S(1)} %collective-permute-done.12.a_ref), channel_id=1, source_target_pairs={{0,32},{4,36},{8,40},{12,44},{16,48},{20,52},{24,56},{28,60},{32,6... | collective-permute-start | bytes 1572872 | tf_op jit(solution)/shard_map/ppermute | solution.py:27
  70.1 15.3 %collective-permute-start.15 = (bf16[2048,128]{1,0:T(8,128)(2,1)S(1)}, bf16[2048,128]{1,0:T(8,128)(2,1)S(1)}, u32[]{:S(2)}, u32[]{:S(2)}) collective-permute-start(bf16[2048,128]{1,0:T(8,128)(2,1)S(1)} %collective-permute-done.13.b_ref), channel_id=1, source_target_pairs={{0,224},{4,228},{8,232},{12,236},{16,240},{20,244},{24,248},{28,25... | collective-permute-start | bytes 1572872 | tf_op jit(solution)/shard_map/ppermute | solution.py:27
  85.5 6.5 %collective-permute-start.16 = (bf16[1024,128]{1,0:T(8,128)(2,1)S(1)}, bf16[1024,128]{1,0:T(8,128)(2,1)S(1)}, u32[]{:S(2)}, u32[]{:S(2)}) collective-permute-start(bf16[1024,128]{1,0:T(8,128)(2,1)S(1)} %slice.327), channel_id=1, source_target_pairs={{0,32},{4,36},{8,40},{12,44},{16,48},{20,52},{24,56},{28,60},{32,6... | collective-permute-start | bytes 786440 | tf_op jit(solution)/shard_map/ppermute | solution.py:27
  85.6 6.5 %collective-permute-start.17 = (bf16[1024,128]{1,0:T(8,128)(2,1)S(1)}, bf16[1024,128]{1,0:T(8,128)(2,1)S(1)}, u32[]{:S(2)}, u32[]{:S(2)}) collective-permute-start(bf16[1024,128]{1,0:T(8,128)(2,1)S(1)} %slice.328), channel_id=1, source_target_pairs={{0,224},{4,228},{8,232},{12,236},{16,240},{20,244},{24,248},{28,25... | collective-permute-start | bytes 786440 | tf_op jit(solution)/shard_map/ppermute | solution.py:27
  101.0 3.8 %collective-permute-start.19 = (f32[12,128,256]{2,1,0:T(8,128)}, f32[12,128,256]{2,1,0:T(8,128)}, u32[]{:S(2)}, u32[]{:S(2)}) collective-permute-start(f32[12,128,256]{2,1,0:T(8,128)} %get-tuple-element.95), channel_id=1, source_target_pairs={{0,4},{4,0},{8,12},{12,8},{16,20},{20,16},{24,28},{28,24},{32,36},... | collective-permute-start | bytes 4718600 | tf_op jit(solution)/shard_map/ppermute | solution.py:27
  101.0 3.8 %collective-permute-start.18 = (f32[12,8,256]{2,1,0:T(8,128)S(1)}, f32[12,8,256]{2,1,0:T(8,128)S(1)}, u32[]{:S(2)}, u32[]{:S(2)}) collective-permute-start(f32[12,8,256]{2,1,0:T(8,128)S(1)} %get-tuple-element.94), channel_id=1, source_target_pairs={{0,4},{4,0},{8,12},{12,8},{16,20},{20,16},{24,28},{28,24},{32,36},... | collective-permute-start | bytes 294920 | tf_op jit(solution)/shard_map/ppermute | solution.py:27
  108.2 20.1 %collective-permute-start.20 = (bf16[2,128,256]{2,1,0:T(8,128)(2,1)S(1)}, bf16[2,128,256]{2,1,0:T(8,128)(2,1)S(1)}, u32[]{:S(2)}, u32[]{:S(2)}) collective-permute-start(bf16[2,128,256]{2,1,0:T(8,128)(2,1)S(1)} %get-tuple-element.106), channel_id=1, source_target_pairs={{0,224},{4,228},{8,232},{12,236},{16,240},{20,244},{24,248},{28,25... | collective-permute-start | bytes 393224 | tf_op jit(solution)/shard_map/ppermute | solution.py:419
  132.3 19.1 %all-to-all-start.1 = ((bf16[4,64,2048]{2,1,0:T(8,128)(2,1)}), bf16[4,64,2048]{2,1,0:T(8,128)(2,1)}, u32[]{:S(2)}, u32[]{:S(2)}) async-start(bf16[4,64,2048]{2,1,0:T(8,128)(2,1)} %bitcast.45), calls=%async_computation.1 | async-start | bytes 2097152 | tf_op jit(solution)/shard_map/all_to_all | solution.py:435
  136.6 8.7 %collective-permute-start.21 = (f32[2,2,256]{2,0,1:T(2,128)S(1)}, f32[2,2,256]{2,0,1:T(2,128)S(1)}, u32[]{:S(2)}, u32[]{:S(2)}) collective-permute-start(f32[2,2,256]{2,0,1:T(2,128)S(1)} %copy.42), channel_id=1, source_target_pairs={{0,224},{4,228},{8,232},{12,236},{16,240},{20,244},{24,248},{28,25... | collective-permute-start | bytes 12296 | tf_op jit(solution)/shard_map/ppermute | solution.py:420
  (16 other events, 136.8 us)
